TPU v7x, 512 devices: a whole 4x4x16 slice. The times are simulated.
512 devices in a mesh: sp: 32 (over z, core), tp: 16 (over y, x).
Axes of the slice: x: 4, y: 4, z: 16, core: 2. Of those that a mesh axis runs over, the one named last changes fastest.
Arguments:
- residual_in: bfloat16 [8192, 2048], P('sp', 'tp'), may hold values from -20 to 20
- conv_value: bfloat16 [8192, 2048], P('sp', 'tp'), may hold values from -6 to 6
- conv_gate: bfloat16 [8192, 2048], P('sp', 'tp'), may hold values from -9 to 9
- doc_ids: int32 [8192], P('sp'), may hold values from 0 to 15, never falling along the last dimension, each value on 1 to 1024 neighbouring positions
- conv_kernel: bfloat16 [31, 2048], P(None, 'tp'), may hold values from -3 to 3
- ln_gain: bfloat16 [2048], P('tp'), may hold values from 0.099609375 to 1.8984375
- out_weight: bfloat16 [2048, 2048], P(None, 'tp'), may hold values from -0.25 to 0.25
- norm_gain: bfloat16 [2048], P('tp'), may hold values from 0.099609375 to 1.8984375
- routes: int32 [8192, 2], P('sp'), may hold values from 0 to 31, all different within a row; in each aligned block of 256 rows (0 to 255, 256 to 511, ...) at most 32 rows name the same one
- route_weight: float32 [8192, 2], P('sp'), may hold values from 0.1 to 1
- gate_w: bfloat16 [32, 2048, 4096], P('sp', None, 'tp'), may hold values from -0.125 to 0.125
- up_w: bfloat16 [32, 2048, 4096], P('sp', None, 'tp'), may hold values from -0.125 to 0.125
- down_w: bfloat16 [32, 4096, 2048], P('sp', 'tp'), may hold values from -0.125 to 0.125
Outputs:
- mixed: bfloat16 [8192, 2048], P('sp', 'tp')
Inputs may be any that keep to these rules, and one draw needn't show every extreme that they name: `routes`: in each aligned block of 256 positions no expert is named by more than 32 positions, a bound that some block reaches; a position's two experts differ. `doc_ids`: never falls along the positions; each document spans 1 to 1024 positions, one exactly that many.
All inputs are finite; a program needn't handle non-finite values.
Results may differ from a plain program's by a relative error of at most 0.012.
Values may be sent and summed in bfloat16 or wider, within the bound.
A program may use at most 64 MiB of HBM per device.

v0:
```python
import jax
import jax.numpy as jnp
from jax import lax
from jax.sharding import Mesh
from jax.sharding import PartitionSpec as P

TP = ("tp_0", "tp_1")


epsilon = 1e-06


def from_behind(x, axis, by):
    peers = lax.axis_size(axis)
    pairs = [(i, i + by) for i in range(peers) if 0 <= i + by < peers]
    return lax.ppermute(x, axis, pairs)


def over_axes(x, axes):
    for axis in axes:
        x = lax.psum(x, axis)
    return x


def copy_for_each(x, axis):
    copies = jnp.broadcast_to(x, (lax.axis_size(axis), *x.shape))
    return lax.all_to_all(copies, axis, split_axis=0, concat_axis=0, tiled=True)


def laid_out(pieces, dim):
    lengths = list(pieces.shape[1:])
    lengths[dim] *= pieces.shape[0]
    return jnp.moveaxis(pieces, 0, dim).reshape(lengths)


def collect(x, axis, dim):
    pieces = copy_for_each(x, axis)
    return laid_out(pieces, dim)


def in_blocks(x, dim, peers):
    before, after = (x.shape[:dim], x.shape[dim + 1 :])
    return jnp.moveaxis(x.reshape(*before, peers, -1, *after), dim, 0)


def sum_at_owner(x, axis, dim):
    peers = lax.axis_size(axis)
    pieces = lax.all_to_all(in_blocks(x, dim, peers), axis, 0, 0, tiled=True)
    return jnp.sum(pieces.astype(jnp.float32), axis=0)


def per_device(
    residual_in,
    conv_value,
    conv_gate,
    doc_ids,
    conv_kernel,
    ln_gain,
    out_weight,
    norm_gain,
    routes,
    route_weight,
    gate_w,
    up_w,
    down_w,
):
    rows_here, chan_here = conv_value.shape
    lookback = conv_kernel.shape[0] - 1
    gated = (conv_value.astype(jnp.float32) * jax.nn.sigmoid(conv_gate.astype(jnp.float32))).astype(
        jnp.bfloat16
    )
    tail_values, tail_docs = from_behind(
        (gated[rows_here - lookback :], doc_ids[rows_here - lookback :]), "sp", 1
    )
    extended = jnp.concatenate([tail_values, gated], 0)
    doc_extended = jnp.concatenate([tail_docs, doc_ids], 0)
    kernel = conv_kernel.astype(jnp.float32)
    conv_out = jnp.zeros((rows_here, chan_here), jnp.float32)
    for kernel_tap in range(lookback + 1):
        same_doc = (doc_extended[kernel_tap : kernel_tap + rows_here] == doc_ids)[:, None]
        conv_out = conv_out + jnp.where(
            same_doc,
            extended[kernel_tap : kernel_tap + rows_here].astype(jnp.float32) * kernel[kernel_tap],
            0.0,
        )
    channel_sum, channel_sq = (
        over_axes(jnp.sum(conv_out, 1), TP),
        over_axes(jnp.sum(conv_out * conv_out, 1), TP),
    )
    channels = chan_here * lax.axis_size(TP)
    chan_mean = channel_sum[:, None] / channels
    chan_square = channel_sq[:, None] / channels
    activated = jax.nn.silu(
        (conv_out - chan_mean)
        * lax.rsqrt(chan_square - chan_mean * chan_mean + epsilon)
        * ln_gain.astype(jnp.float32)
    ).astype(jnp.bfloat16)
    projected = jnp.dot(
        collect(activated, TP, 1), out_weight, preferred_element_type=jnp.float32
    ).astype(jnp.bfloat16)
    stream = (residual_in.astype(jnp.float32) + projected.astype(jnp.float32)).astype(jnp.bfloat16)
    columns = stream.shape[1]
    model_width = columns * lax.axis_size(TP)
    experts = lax.axis_size("sp")
    capacity = 4 * rows_here // experts
    flat_routes = routes.reshape(-1)
    onehot = (flat_routes[:, None] == jnp.arange(experts, dtype=jnp.int32)).astype(jnp.int32)
    slot_rank = jnp.sum((jnp.cumsum(onehot, 0) - onehot) * onehot, 1)
    token_of = jnp.arange(rows_here * 2, dtype=jnp.int32) // 2
    slot_token = (
        jnp.full((experts * capacity,), rows_here, jnp.int32)
        .at[flat_routes * capacity + slot_rank]
        .set(token_of)
    )
    stream_part = stream.astype(jnp.float32)
    row_total = over_axes(jnp.sum(stream_part * stream_part, 1), TP)
    normed = (
        stream_part
        * lax.rsqrt(row_total[:, None] / model_width + epsilon)
        * norm_gain.astype(jnp.float32)
    ).astype(jnp.bfloat16)
    outbound = jnp.take(normed, slot_token, axis=0, mode="fill", fill_value=0).reshape(
        experts, capacity, columns
    )
    received = collect(
        lax.all_to_all(outbound, "sp", split_axis=0, concat_axis=0, tiled=True), TP, 2
    )
    sources, slots, features = received.shape
    gathered = received.reshape(sources * slots, features)
    hidden = (
        jax.nn.silu(jnp.dot(gathered, gate_w[0], preferred_element_type=jnp.float32))
        * jnp.dot(gathered, up_w[0], preferred_element_type=jnp.float32)
    ).astype(jnp.bfloat16)
    partial_value = jnp.dot(hidden, down_w[0], preferred_element_type=jnp.float32)
    partial_value = (
        lax.optimization_barrier(partial_value.astype(jnp.bfloat16))
        .astype(jnp.float32)
        .reshape(sources, slots, features)
    )
    summed = sum_at_owner(partial_value.astype(jnp.bfloat16), TP, 2).astype(jnp.bfloat16)
    returned = lax.all_to_all(summed, "sp", split_axis=0, concat_axis=0, tiled=True)
    pick_index = flat_routes * capacity + slot_rank
    picked = jnp.take(returned.reshape(-1, columns), pick_index, axis=0).reshape(
        rows_here, 2, columns
    )
    routed = jnp.sum(picked.astype(jnp.float32) * route_weight[:, :, None], 1)
    return (stream.astype(jnp.float32) + routed).astype(jnp.bfloat16)


def solution(mesh):
    split = Mesh(mesh.devices.reshape(mesh.shape["sp"], 4, 4), ("sp", "tp_0", "tp_1"))
    in_specs = (
        P("sp", TP),
        P("sp", TP),
        P("sp", TP),
        P("sp"),
        P(None, TP),
        P(TP),
        P(None, TP),
        P(TP),
        P("sp", None),
        P("sp", None),
        P("sp", None, TP),
        P("sp", None, TP),
        P("sp", TP, None),
    )
    out_specs = P("sp", TP)
    return jax.shard_map(
        per_device, mesh=split, in_specs=in_specs, out_specs=out_specs, check_vma=False
    )
```

profile of v0, /device:TPU:1, one launch (start us, length us, event | category | flops | bytes accessed | tf_op | source)
XLA Modules:
  0.0 283.4 jit_solution(12368834706082618189)
XLA Ops:
  0.0 0.9 slice.285
  0.9 4.9 %collective-permute-start = (s32[30]{0:T(128)S(1)}, s32[30]{0:T(128)S(1)}, u32[]{:S(2)}, u32[]{:S(2)}) collective-permute-start(s32[30]{0:T(128)S(1)} %slice.285), channel_id=1, source_target_pairs={{0,16},{16,32},{32,48},{48,64},{64,80},{80,96},{96,112},{112,128},... | collective-permute-start | bytes 368 | tf_op jit(solution)/shard_map/ppermute | solution.py:16
  5.8 0.9 multiply_convert_fusion.2
  6.7 1.9 collective-permute-start.1
  8.7 0.7 convert_element_type.165
  9.4 0.8 copy.42
  10.2 0.1 eq.146
  10.5 0.7 broadcast_multiply_fusion
  11.2 0.7 convert_element_type.196
  11.8 0.9 copy.40
  12.8 0.7 convert_element_type.204
  13.5 1.2 reduce-window.6
  14.6 0.8 pad_add_fusion
  15.4 0.8 slice_compare_fusion.29
  16.2 0.8 slice_compare_fusion.28
  16.9 1.9 fusion.68
  18.8 8.7 %all-reduce.1 = (f32[256]{0:T(256)S(1)}, f32[256]{0:T(256)S(1)}) all-reduce(f32[256]{0:T(256)S(1)} %get-tuple-element.6, f32[256]{0:T(256)S(1)} %get-tuple-element.5), channel_id=1, replica_groups=mesh['sp'=32,'tp_0'=4,'tp_1'=4] {'tp_0'}, use_global_device_ids=true, to_apply=%region_4.5 | all-reduce | flops 512 | bytes 4096 | tf_op jit(solution)/shard_map/psum | solution.py:21
  27.6 8.6 %all-reduce = (f32[256]{0:T(256)S(1)}, f32[256]{0:T(256)S(1)}) all-reduce(f32[256]{0:T(256)S(1)} %get-tuple-element.9, f32[256]{0:T(256)S(1)} %get-tuple-element.10), channel_id=1, replica_groups=mesh['sp'=32,'tp_0'=4,'tp_1'=4] {'tp_1'}, use_global_device_ids=true, to_apply=%region_5.6 | all-reduce | flops 512 | bytes 4096 | tf_op jit(solution)/shard_map/psum | solution.py:21
  36.2 0.2 multiply_convert_fusion.1
  36.4 1.1 broadcast_in_dim.293
  37.5 3.7 %all-to-all-start = ((bf16[16,256,128]{1,2,0:T(8,128)(2,1)}), bf16[16,256,128]{1,2,0:T(8,128)(2,1)S(1)}, u32[]{:S(2)}, u32[]{:S(2)}) async-start(bf16[16,256,128]{1,2,0:T(8,128)(2,1)} %broadcast_in_dim.293), calls=%async_computation | async-start | bytes 2097152 | tf_op jit(solution)/shard_map/all_to_all | solution.py:27
  41.2 0.2 slice_reduce_fusion
  41.5 0.1 copy.47
  41.6 0.1 mul.497
  41.9 2.4 scatter_custom_fusion
  44.4 10.3 %all-to-all-done = bf16[16,256,128]{1,2,0:T(8,128)(2,1)S(1)} async-done(((bf16[16,256,128]{1,2,0:T(8,128)(2,1)}), bf16[16,256,128]{1,2,0:T(8,128)(2,1)S(1)}, u32[]{:S(2)}, u32[]{:S(2)}) %all-to-all-start) | async-done | bytes 1048608 | tf_op jit(solution)/shard_map/all_to_all | solution.py:27
  54.7 0.4 multiply_reduce_fusion.1
  55.1 7.0 %psum.46 = f32[256]{0:T(256)S(1)} all-reduce(f32[256]{0:T(256)S(1)} %get-tuple-element.75), channel_id=1, replica_groups=mesh['sp'=32,'tp_0'=4,'tp_1'=4] {'tp_0'}, use_global_device_ids=true, to_apply=%region_11.12 | all-reduce | flops 256 | bytes 2048 | tf_op jit(solution)/shard_map/psum | solution.py:21
  62.1 6.0 %psum.47 = f32[256]{0:T(256)S(1)} all-reduce(f32[256]{0:T(256)S(1)} %psum.46), channel_id=1, replica_groups=mesh['sp'=32,'tp_0'=4,'tp_1'=4] {'tp_1'}, use_global_device_ids=true, to_apply=%region_12.13 | all-reduce | flops 256 | bytes 2048 | tf_op jit(solution)/shard_map/psum | solution.py:21
  68.3 3.2 %gather_fusion = bf16[1024,128]{1,0:T(8,128)(2,1)S(1)} fusion(bf16[256,128]{1,0:T(8,128)(2,1)S(1)} %copy.48, s32[1024]{0:T(1024)S(1)} %fusion.61), kind=kCustom, calls=%fused_computation | custom fusion | bytes 528384 | tf_op jit(solution)/shard_map/jit(_take)/gather | solution.py:122
  71.5 0.2 broadcast_select_fusion
  71.7 45.7 %all_to_all.25 = bf16[32,32,128]{2,1,0:T(8,128)(2,1)S(1)} all-to-all(bf16[32,32,128]{2,1,0:T(8,128)(2,1)S(1)} %broadcast_select_fusion), channel_id=1, replica_groups=mesh['sp'=32,'tp_0'=4,'tp_1'=4] {'sp'}, dimensions={0} | all-to-all | bytes 524288 | tf_op jit(solution)/shard_map/all_to_all | solution.py:126
  117.4 0.8 broadcast_in_dim.300
  118.2 52.5 %all_to_all.26 = bf16[16,32,32,128]{3,2,1,0:T(8,128)(2,1)S(1)} all-to-all(bf16[16,32,32,128]{3,2,1,0:T(8,128)(2,1)S(1)} %broadcast_in_dim.300), channel_id=1, replica_groups=mesh['sp'=32,'tp_0'=4,'tp_1'=4] {'tp_0','tp_1'}, dimensions={0} | all-to-all | bytes 8388608 | tf_op jit(solution)/shard_map/all_to_all | solution.py:27
  170.7 4.9 %copy.49 = bf16[32,32,16,128]{3,2,1,0:T(8,128)(2,1)S(1)} copy(bf16[32,32,16,128]{3,1,0,2:T(8,128)(2,1)S(1)} %bitcast.121) | data formatting | bytes 8388608 | tf_op jit(solution)/shard_map/transpose | solution.py:33
  175.6 1.9 copy-done.1
  177.5 2.3 fusion.2
  179.8 8.8 %convolution_convert_fusion = bf16[1024,2048]{1,0:T(8,128)(2,1)} fusion(bf16[128,8,16,128]{3,2,1,0:T(8,128)(2,1)} %bitcast.126, bf16[1,256,2048]{2,1,0:T(8,128)(2,1)S(1)} %copy-done, bf16[1,2048,256]{2,1,0:T(8,128)(2,1)S(1)} %copy-done.6, f32[1024,256]{1,0:T(8,128)} %fusion.2), kind=kOutput, calls=%fused_computation.8 | convolution fusion | flops 2151153664 | bytes 11534336 | tf_op jit(solution)/shard_map/dot_general | solution.py:134
  188.6 3.6 %copy.56 = bf16[128,8,16,128]{3,2,1,0:T(8,128)(2,1)S(1)} copy(bf16[128,8,16,128]{3,1,2,0:T(8,128)(2,1)} %bitcast.127) | data formatting | bytes 8388608
  192.2 1.3 copy.73
  193.5 53.1 %all_to_all.27 = bf16[16,32,32,128]{3,2,1,0:T(8,128)(2,1)} all-to-all(bf16[16,32,32,128]{3,2,1,0:T(8,128)(2,1)S(1)} %bitcast.123), channel_id=1, replica_groups=mesh['sp'=32,'tp_0'=4,'tp_1'=4] {'tp_0','tp_1'}, dimensions={0} | all-to-all | bytes 8388608 | tf_op jit(solution)/shard_map/all_to_all | solution.py:48
  246.7 3.5 %reduce_sum.67 = bf16[32,32,128]{2,1,0:T(8,128)(2,1)} reduce(bf16[16,32,32,128]{3,2,1,0:T(8,128)(2,1)} %all_to_all.27, bf16[]{:T(256)} %constant.71.clone.1), dimensions={0}, to_apply=%region_13.14 | reduce | flops 1966080 | bytes 4456450 | tf_op jit(solution)/shard_map/reduce_sum | solution.py:49
  250.2 7.2 %all-to-all-start.4 = ((bf16[32,32,128]{2,1,0:T(8,128)(2,1)}), bf16[32,32,128]{2,1,0:T(8,128)(2,1)S(1)}, u32[]{:S(2)}, u32[]{:S(2)}) async-start(bf16[32,32,128]{2,1,0:T(8,128)(2,1)} %reduce_sum.67), calls=%async_computation.4 | async-start | bytes 524288 | tf_op jit(solution)/shard_map/all_to_all | solution.py:141
  257.7 0.2 copy.46
  258.0 21.7 %all-to-all-done.4 = bf16[32,32,128]{2,1,0:T(8,128)(2,1)S(1)} async-done(((bf16[32,32,128]{2,1,0:T(8,128)(2,1)}), bf16[32,32,128]{2,1,0:T(8,128)(2,1)S(1)}, u32[]{:S(2)}, u32[]{:S(2)}) %all-to-all-start.4) | async-done | bytes 262176 | tf_op jit(solution)/shard_map/all_to_all | solution.py:141
  279.7 1.3 gather_fusion.1
  281.0 1.5 multiply_reduce_fusion
  282.6 0.7 copy.53
  (40 shorter events, 1.3 us)
Async XLA Ops:
  0.0 179.8 %copy-start = (bf16[1,256,2048]{2,1,0:T(8,128)(2,1)S(1)}, bf16[1,256,2048]{2,1,0:T(8,128)(2,1)}, u32[]{:S(2)}) copy-start(bf16[1,256,2048]{2,1,0:T(8,128)(2,1)} %param.25) | copy-start | bytes 3145732
  0.0 54.7 %copy-start.2 = (bf16[2048,128]{1,0:T(8,128)(2,1)S(1)}, bf16[2048,128]{1,0:T(8,128)(2,1)}, u32[]{:S(2)}) copy-start(bf16[2048,128]{1,0:T(8,128)(2,1)} %param.19) | copy-start | bytes 1572868
  0.9 13.8 %collective-permute-start = (s32[30]{0:T(128)S(1)}, s32[30]{0:T(128)S(1)}, u32[]{:S(2)}, u32[]{:S(2)}) collective-permute-start(s32[30]{0:T(128)S(1)} %slice.285), channel_id=1, source_target_pairs={{0,16},{16,32},{32,48},{48,64},{64,80},{80,96},{96,112},{112,128},... | collective-permute-start | bytes 368 | tf_op jit(solution)/shard_map/ppermute | solution.py:16
  6.7 10.2 %collective-permute-start.1 = (bf16[30,128]{1,0:T(8,128)(2,1)S(1)}, bf16[30,128]{1,0:T(8,128)(2,1)S(1)}, u32[]{:S(2)}, u32[]{:S(2)}) collective-permute-start(bf16[30,128]{1,0:T(8,128)(2,1)S(1)} %slice.384), channel_id=1, source_target_pairs={{0,16},{16,32},{32,48},{48,64},{64,80},{80,96},{96,112},{112,128},... | collective-permute-start | bytes 23048 | tf_op jit(solution)/shard_map/ppermute | solution.py:16
  37.5 17.2 %all-to-all-start = ((bf16[16,256,128]{1,2,0:T(8,128)(2,1)}), bf16[16,256,128]{1,2,0:T(8,128)(2,1)S(1)}, u32[]{:S(2)}, u32[]{:S(2)}) async-start(bf16[16,256,128]{1,2,0:T(8,128)(2,1)} %broadcast_in_dim.293), calls=%async_computation | async-start | bytes 2097152 | tf_op jit(solution)/shard_map/all_to_all | solution.py:27
  170.7 6.8 %copy-start.5 = (bf16[1,2048,256]{2,1,0:T(8,128)(2,1)S(1)}, bf16[1,2048,256]{2,1,0:T(8,128)(2,1)}, u32[]{:S(2)}) copy-start(bf16[1,2048,256]{2,1,0:T(8,128)(2,1)} %param.23) | copy-start | bytes 3145732
  175.6 1.9 copy-start.1
  177.5 2.3 copy-start.6
  246.6 11.0 %copy-start.3 = (s32[256,2]{0,1:T(2,128)S(1)}, s32[256,2]{0,1:T(2,128)}, u32[]{:S(2)}) copy-start(s32[256,2]{0,1:T(2,128)} %param.21) | copy-start | bytes 6148
  246.7 11.2 %copy-start.4 = (f32[256,2]{0,1:T(2,128)S(1)}, f32[256,2]{0,1:T(2,128)}, u32[]{:S(2)}) copy-start(f32[256,2]{0,1:T(2,128)} %param.22) | copy-start | bytes 6148
  250.2 29.5 %all-to-all-start.4 = ((bf16[32,32,128]{2,1,0:T(8,128)(2,1)}), bf16[32,32,128]{2,1,0:T(8,128)(2,1)S(1)}, u32[]{:S(2)}, u32[]{:S(2)}) async-start(bf16[32,32,128]{2,1,0:T(8,128)(2,1)} %reduce_sum.67), calls=%async_computation.4 | async-start | bytes 524288 | tf_op jit(solution)/shard_map/all_to_all | solution.py:141
where the time goes:
time: 284 us; the launch traced here: 283 us
  blocking collectives  182 us (64%)
  waiting for transfers between devices  32 us (11%)
  local copies, waits for them, and re-layouts  25.6 us (9%)
  starting transfers between devices  17.7 us (6%)
  other arithmetic  14.6 us (5%)
  matrix products  11.5 us (4%)
    all_to_all x1, blocking collectives, sum_at_owner(): pieces = lax.all_to_all(in_blocks(x, dim, peers), axis, 0, 0, tiled=True)  53.1 us
    all_to_all x1, blocking collectives, copy_for_each(): return lax.all_to_all(copies, axis, split_axis=0, concat_axis=0, tiled=True)  52.5 us
    all_to_all x1, blocking collectives, per_device(): lax.all_to_all(outbound, 'sp', split_axis=0, concat_axis=0, tiled=True)  45.7 us
    psum x4, blocking collectives, over_axes(): x = lax.psum(x, axis)  30.3 us
    all_to_all x1, waiting for transfers between devices, per_device(): lax.all_to_all(summed, 'sp', split_axis=0, concat_axis=0, tiled=True)  21.7 us
    all_to_all x1, waiting for transfers between devices, copy_for_each(): return lax.all_to_all(copies, axis, split_axis=0, concat_axis=0, tiled=True)  10.3 us
    dot_general x1, matrix products, per_device(): jnp.dot(hidden, down_w[0], preferred_element_type=jnp.float32)  8.8 us
    unnamed x18, local copies, waits for them, and re-layouts  7.4 us
  transfers between devices with their start and end apart: 4, of which 2 were waited for; matrix products, arithmetic and copies ran while one was open for 5% of the time, Pallas kernels for 0%

commit v1 on v0

v1 whole, which is shorter than its diff:
```python
import functools

import jax
import jax.numpy as jnp
from jax import lax
from jax.experimental import pallas as pl
from jax.experimental.pallas import tpu as pltpu
from jax.sharding import Mesh
from jax.sharding import PartitionSpec as P

MESH = pl.DeviceIdType.MESH
F32 = jnp.float32
BF16 = jnp.bfloat16
AXES = ("z", "core", "y", "x")
TP = ("y", "x")
SP = ("z", "core")
EPS = 1e-06

ROWS = 256
LANES = 128
RING = 4
NTP = RING * RING
WIDE = RING * LANES
FULL = NTP * LANES
TAPS = 31
HALO = 32
EXPERTS = 32
CAP = 32
SLOTS = EXPERTS * CAP
NZ = 16
G1 = 2
G2 = 4
R1 = ROWS // G1 // 2
R2 = SLOTS // G2 // 2
CHUNKS = R2 // CAP
ZFIRST = 4


def remote(src, dst, send, recv, dev):
    return pltpu.make_async_remote_copy(
        src_ref=src,
        dst_ref=dst,
        send_sem=send,
        recv_sem=recv,
        device_id=dev,
        device_id_type=MESH,
    )


def distance(i):
    k = lax.rem(i + ZFIRST, NZ)
    half = (k + 1) // 2
    return jnp.where(lax.rem(k, 2) == 1, half, NZ - half)


def to_column(row):
    return jnp.transpose(jnp.broadcast_to(row, (LANES, row.shape[1])))


def true_block(part, pos):
    return pos if part == 0 else (pos % RING) * RING + pos // RING


def kernel(
    cv,
    cg,
    doc,
    ck,
    lng,
    res,
    routes,
    rw,
    ng,
    ow_hbm,
    gw_hbm,
    uw_hbm,
    dw_hbm,
    out,
    ow,
    gw,
    uw,
    dw,
    ext,
    docx,
    hg_out,
    hd_out,
    hg_in,
    hd_in,
    conv,
    stat,
    gains,
    colstat,
    xg,
    act,
    strm,
    pick,
    dsp,
    x2g,
    nrm,
    hid,
    part_sum,
    t1,
    u1,
    v1,
    s1,
    q1,
    t2,
    u2,
    v2,
    s2,
    fin,
    ret,
    wsem,
    hsend,
    hrecv,
    stsend,
    strecv,
    ssem1,
    rsem1,
    ssem2,
    rsem2,
    dsend,
    drecv,
    rsend,
    rrecv,
):
    z = lax.axis_index("z")
    c = lax.axis_index("core")
    y = lax.axis_index("y")
    x = lax.axis_index("x")
    me_tp = y * RING + x
    me_sp = z * 2 + c

    weights = [
        pltpu.make_async_copy(src, dst, wsem.at[i])
        for i, (src, dst) in enumerate(
            ((ow_hbm, ow), (gw_hbm.at[0], gw), (uw_hbm.at[0], uw), (dw_hbm.at[0], dw))
        )
    ]
    for w in weights:
        w.start()

    barrier = pltpu.get_barrier_semaphore()

    def tp_peer(k):
        other = lax.rem(me_tp + k, NTP)
        return (z, c, other // RING, lax.rem(other, RING))

    def sp_peer(k):
        other = lax.rem(me_sp + k, 2 * NZ)
        return (other // 2, lax.rem(other, 2), y, x)

    def greet_tp(k, carry):
        pl.semaphore_signal(barrier, inc=1, device_id=tp_peer(k), device_id_type=MESH)
        return carry

    def greet_sp(k, carry):
        pl.semaphore_signal(barrier, inc=1, device_id=sp_peer(k), device_id_type=MESH)
        return carry

    lax.fori_loop(1, 2 * NZ, greet_sp, 0)
    lax.fori_loop(1, NTP, greet_tp, 0)

    gate = cg[...].astype(F32)
    gated = (cv[...].astype(F32) * (1.0 / (1.0 + jnp.exp(-gate)))).astype(BF16)
    ext[HALO:, :] = gated.astype(F32)
    hg_out[...] = gated[ROWS - HALO :, :]
    dcol = to_column(doc[...].astype(F32))
    docx[HALO:, :] = dcol
    hd_out[...] = dcol[ROWS - HALO :, :]
    taps = ck[...].astype(F32)

    def conv_rows(first, count):
        acc = jnp.zeros((count, LANES), F32)
        mine = docx[HALO + first : HALO + first + count, :]
        for tap in range(TAPS):
            at = HALO + first - (TAPS - 1) + tap
            same = docx[at : at + count, :] == mine
            term = ext[at : at + count, :] * taps[tap : tap + 1, :]
            acc = acc + jnp.where(same, term, 0.0)
        conv[first : first + count, :] = acc

    for first in range(HALO, ROWS, 32):
        conv_rows(first, 32)

    pl.semaphore_wait(barrier, NTP - 1 + 2 * NZ - 1)

    after = sp_peer(1)
    halo_g = remote(hg_out, hg_in, hsend.at[0], hrecv.at[0], after)
    halo_d = remote(hd_out, hd_in, hsend.at[1], hrecv.at[1], after)
    halo_g.start()
    halo_d.start()

    ids = routes[...]
    expert = lax.broadcasted_iota(jnp.int32, (EXPERTS, ROWS), 0)
    names = [(expert == ids[k : k + 1, :]).astype(F32) for k in range(2)]
    before = (
        lax.broadcasted_iota(jnp.int32, (ROWS, ROWS), 0)
        < lax.broadcasted_iota(jnp.int32, (ROWS, ROWS), 1)
    ).astype(F32)
    earlier = jnp.dot(
        (names[0] + names[1]).astype(BF16), before.astype(BF16), preferred_element_type=F32
    )
    slot_base = expert.astype(F32) * float(CAP)
    slots = [jnp.sum(n * (earlier + slot_base), axis=0, keepdims=True) for n in names]
    lane = lax.broadcasted_iota(jnp.int32, (ROWS, LANES), 1).astype(F32)
    for k in range(2):
        col = to_column(slots[k])
        for b in range(SLOTS // LANES):
            pick[k, :, b * LANES : (b + 1) * LANES] = (
                (lane + float(b * LANES)) == col
            ).astype(BF16)

    halo_g.wait()
    halo_d.wait()
    first_block = me_sp == 0
    ext[:HALO, :] = hg_in[...].astype(F32)
    docx[:HALO, :] = jnp.where(first_block, -1.0, hd_in[...])
    conv_rows(0, HALO)

    cx = conv[...]
    cxt = jnp.transpose(cx)
    local = jnp.sum(cxt, axis=0, keepdims=True) * (1.0 / LANES)
    spread = cxt - local
    second = jnp.sum(spread * spread, axis=0, keepdims=True)
    gain_row = jnp.concatenate([lng[...].astype(F32), ng[...].astype(F32)], axis=1)
    stat[me_tp] = jnp.concatenate(
        [local, second, gain_row, jnp.zeros((5, ROWS), F32)], axis=0
    )
    dev = (cx - to_column(local)).astype(BF16)
    for g in range(G1):
        for part in range(2):
            mm, mj = (x, y) if part == 0 else (y, x)
            lo = g * 2 * R1 + part * R1
            pos = pl.multiple_of((mj * RING + mm) * LANES, LANES)
            xg[lo : lo + R1, pl.ds(pos, LANES)] = dev[lo : lo + R1, :]

    def send_stat(k, carry):
        remote(stat.at[me_tp], stat.at[me_tp], stsend.at[k], strecv.at[k], tp_peer(k)).start()
        return carry

    def ring(part, g, rows, first):
        mm, mj = (x, y) if part == 0 else (y, x)
        step = 1 - 2 * (g % 2) if isinstance(g, int) else 1 - 2 * lax.rem(g, 2)

        def at(base, by):
            return lax.rem(base + by * step + 2 * RING, RING)

        def minor(by):
            m = at(mm, by)
            return (z, c, mj, m) if part == 0 else (z, c, m, mj)

        def major(by):
            m = at(mj, by)
            return (z, c, m, mm) if part == 0 else (z, c, mm, m)

        def block(by):
            return pl.ds(pl.multiple_of((mj * RING + at(mm, by)) * LANES, LANES), LANES)

        def wide(by):
            return pl.ds(pl.multiple_of(at(mj, by) * WIDE, WIDE), WIDE)

        def small(by):
            return pl.ds(pl.multiple_of(at(mm, by) * LANES, LANES), LANES)

        lo = pl.multiple_of(first(g, part), rows)
        return minor, major, block, wide, small, pl.ds(lo, rows)

    def make_gather(buf, rows, first, ssem, rsem):
        def move(g, part, kind, cols, dev):
            r = pl.ds(pl.multiple_of(first(g, part), rows), rows)
            ref = buf.at[r, cols]
            return remote(ref, ref, ssem.at[part, kind], rsem.at[g, part, kind], dev)

        def send(g, part, kind, cols, dev):
            d = move(g, part, kind, cols, dev)

            if isinstance(g, int):
                if g > 0:
                    d.wait_send()
            else:
                pl.when(g > 0)(d.wait_send)
            d.start()

        def s0(g):
            for part in range(2):
                minor, _, block, _, _, _ = ring(part, g, rows, first)
                send(g, part, 0, block(0), minor(1))
                send(g, part, 1, block(0), minor(-1))

        def s1(g):
            for part in range(2):
                minor, _, block, _, _, _ = ring(part, g, rows, first)
                move(g, part, 0, block(-1), minor(1)).wait_recv()
                send(g, part, 2, block(-1), minor(1))

        def s2(g):
            for part in range(2):
                minor, major, block, wide, _, _ = ring(part, g, rows, first)
                move(g, part, 1, block(1), minor(1)).wait_recv()
                move(g, part, 2, block(2), minor(1)).wait_recv()
                send(g, part, 3, wide(0), major(1))
                send(g, part, 4, wide(0), major(-1))

        def s3(g):
            for part in range(2):
                _, major, _, wide, _, _ = ring(part, g, rows, first)
                move(g, part, 3, wide(-1), major(1)).wait_recv()
                send(g, part, 5, wide(-1), major(1))

        def s4(g):
            for part in range(2):
                _, major, _, wide, _, _ = ring(part, g, rows, first)
                move(g, part, 4, wide(1), major(1)).wait_recv()
                move(g, part, 5, wide(2), major(1)).wait_recv()

        def drain():
            for part in range(2):
                minor, major, block, wide, _, _ = ring(part, 0, rows, first)
                for kind in range(3):
                    move(0, part, kind, block(0), minor(1)).wait_send()
                for kind in range(3, 6):
                    move(0, part, kind, wide(0), major(1)).wait_send()

        return s0, s1, s2, s3, s4, drain

    def pipeline(stages, groups):
        last = max(d for d, _ in stages)

        def step(t, carry):
            for delay, stage in stages:
                g = t - delay

                @pl.when((g >= 0) & (g < groups))
                def _(stage=stage, g=g):
                    stage(g)

            return carry

        lax.fori_loop(0, groups + last, step, 0)

    def first1(g, part):
        return g * 2 * R1 + part * R1

    a0, a1, a2, a3, a4, adrain = make_gather(xg, R1, first1, ssem1, rsem1)
    for g in range(G1):
        a0(g)
    lax.fori_loop(1, NTP, send_stat, 0)
    pipeline(((4, a4), (3, a3), (2, a2), (1, a1)), G1)

    def wait_stat(k, carry):
        d = remote(stat.at[me_tp], stat.at[me_tp], stsend.at[k], strecv.at[k], tp_peer(k))
        d.wait_send()
        d.wait_recv()
        return carry

    lax.fori_loop(1, NTP, wait_stat, 0)
    adrain()

    means = [stat[j, 0:1, :] for j in range(NTP)]
    mean = sum(means) * (1.0 / NTP)
    shifts = [m - mean for m in means]
    var = (
        sum(stat[j, 1:2, :] for j in range(NTP)) * (1.0 / FULL)
        + sum(s * s for s in shifts) * (1.0 / NTP)
    )
    scale = lax.rsqrt(var + EPS)
    table = jnp.concatenate(shifts + [scale] + [jnp.zeros((LANES - NTP - 1, ROWS), F32)], axis=0)
    colstat[...] = jnp.transpose(table)
    for j in range(NTP):
        gains[:, j * LANES : (j + 1) * LANES] = jnp.concatenate(
            [stat[j, 2:3, :LANES], stat[j, 2:3, LANES:], jnp.zeros((6, LANES), F32)], axis=0
        )

    for part in range(2):

        def normalise(i, carry, part=part):
            g = i // (R1 // 16)
            lo = pl.multiple_of(first1(g, part) + lax.rem(i, R1 // 16) * 16, 16)
            cs = colstat[pl.ds(lo, 16), :]
            rs = cs[:, NTP : NTP + 1]
            for pos in range(NTP):
                j = true_block(part, pos)
                v = xg[pl.ds(lo, 16), pos * LANES : (pos + 1) * LANES].astype(F32)
                v = (v + cs[:, j : j + 1]) * rs * gains[0:1, j * LANES : (j + 1) * LANES]
                v = v / (1.0 + jnp.exp(-v))
                act[pl.ds(lo, 16), j * LANES : (j + 1) * LANES] = v.astype(BF16)
            return carry

        lax.fori_loop(0, G1 * R1 // 16, normalise, 0)

    weights[0].wait()
    projected = jnp.dot(act[...], ow[...], preferred_element_type=F32).astype(BF16)
    strm[...] = (res[...].astype(F32) + projected.astype(F32)).astype(BF16)

    slot = lax.broadcasted_iota(jnp.int32, (SLOTS, ROWS), 0).astype(F32)
    chosen = ((slot == slots[0]) | (slot == slots[1])).astype(BF16)
    dsp[...] = (
        jnp.dot(chosen, strm[...], preferred_element_type=F32)
        .astype(BF16)
        .reshape(EXPERTS, CAP, LANES)
    )

    pos_a = pl.multiple_of((y * RING + x) * LANES, LANES)
    pos_b = pl.multiple_of((x * RING + y) * LANES, LANES)

    def own_pos(r):
        return pl.multiple_of(jnp.where(lax.rem(r // CHUNKS, 2) == 0, pos_a, pos_b), LANES)

    r_self = ((NZ - ZFIRST) % NZ) * 2
    g_self, part_self = r_self // (2 * CHUNKS), (r_self // CHUNKS) % 2

    def dispatch(r, turn):
        dz = distance(r // 2)
        zt = lax.rem(z - dz + NZ, NZ)
        ct = lax.rem(c + r, 2)
        lo = pl.multiple_of(r * CAP, CAP)
        return remote(
            dsp.at[zt * 2 + ct],
            x2g.at[pl.ds(lo, CAP), pl.ds(own_pos(r), LANES)],
            dsend,
            drecv.at[r // CHUNKS],
            (zt, ct, y, x),
        )

    def send_dispatch(r, carry):
        @pl.when(r != r_self)
        def _():
            dispatch(r, 0).start()

        return carry

    lax.fori_loop(0, EXPERTS, send_dispatch, 0)
    x2g[r_self * CAP : (r_self + 1) * CAP, pl.ds(own_pos(jnp.int32(r_self)), LANES)] = dsp[me_sp]

    def first2(g, part):
        return g * 2 * R2 + part * R2

    b0, b1, b2, b3, b4, bdrain = make_gather(x2g, R2, first2, ssem2, rsem2)

    def arrivals(g):
        for part in range(2):
            pos = pos_a if part == 0 else pos_b
            lo = pl.multiple_of(first2(g, part), R2)
            sem = drecv.at[g * 2 + part]
            full = x2g.at[pl.ds(lo, R2), pl.ds(pos, LANES)]
            less = x2g.at[pl.ds(lo, R2 - CAP), pl.ds(pos, LANES)]
            if part == part_self:

                @pl.when(g == g_self)
                def _():
                    pltpu.make_async_copy(less, less, sem).wait()

                @pl.when(g != g_self)
                def _():
                    pltpu.make_async_copy(full, full, sem).wait()
            else:
                pltpu.make_async_copy(full, full, sem).wait()

    def first_stage(g):
        arrivals(g)
        b0(g)

    for w in weights[1:]:
        w.wait()

    def exchange(g, part, kind, src, dst, dev):
        return remote(src, dst, ssem2.at[part, kind], rsem2.at[g, part, kind], dev)

    def push(g, d):
        @pl.when(g > 0)
        def _():
            d.wait_send()

        d.start()

    def expert_stage(g):
        b4(g)
        base = pl.multiple_of(g * 2 * R2, 2 * R2)
        for part in range(2):

            def norm_rows(i, carry, part=part):
                lo = pl.multiple_of(base + part * R2 + i * 16, 16)
                to = pl.multiple_of(part * R2 + i * 16, 16)
                vals = [
                    x2g[pl.ds(lo, 16), pos * LANES : (pos + 1) * LANES].astype(F32)
                    for pos in range(NTP)
                ]
                total = sum(v * v for v in vals)
                rs = lax.rsqrt(jnp.sum(total, axis=1, keepdims=True) * (1.0 / FULL) + EPS)
                for pos in range(NTP):
                    j = true_block(part, pos)
                    nrm[pl.ds(to, 16), j * LANES : (j + 1) * LANES] = (
                        vals[pos] * rs * gains[1:2, j * LANES : (j + 1) * LANES]
                    ).astype(BF16)
                return carry

            lax.fori_loop(0, R2 // 16, norm_rows, 0)
        hg = jnp.dot(nrm[...], gw[...], preferred_element_type=F32)
        hu = jnp.dot(nrm[...], uw[...], preferred_element_type=F32)
        hid[...] = ((hg / (1.0 + jnp.exp(-hg))) * hu).astype(BF16)
        for q in range(RING):
            p = jnp.dot(
                hid[...], dw[:, q * WIDE : (q + 1) * WIDE], preferred_element_type=F32
            ).astype(BF16)
            part_sum[pl.ds(base, R2), q * WIDE : (q + 1) * WIDE] = p[:R2, :]
            for i in range(RING):
                at = (i * RING + q) * LANES
                part_sum[pl.ds(base + R2, R2), at : at + LANES] = p[
                    R2:, i * LANES : (i + 1) * LANES
                ]
        for part in range(2):
            _, major, _, wide, _, r = ring(part, g, R2, first2)
            push(g, exchange(g, part, 6, part_sum.at[r, wide(2)], t1.at[r], major(1)))
            push(g, exchange(g, part, 7, part_sum.at[r, wide(-1)], v1.at[r], major(-1)))

    def c5(g):
        for part in range(2):
            _, major, _, wide, _, r = ring(part, g, R2, first2)
            exchange(g, part, 6, t1.at[r], t1.at[r], major(1)).wait_recv()
            s1[r, :] = (t1[r, :].astype(F32) + part_sum[r, wide(1)].astype(F32)).astype(BF16)
            push(g, exchange(g, part, 8, s1.at[r], u1.at[r], major(1)))

    def c6(g):
        for part in range(2):
            minor, major, _, wide, small, r = ring(part, g, R2, first2)
            exchange(g, part, 7, v1.at[r], v1.at[r], major(1)).wait_recv()
            exchange(g, part, 8, u1.at[r], u1.at[r], major(1)).wait_recv()
            q1[r, :] = (
                part_sum[r, wide(0)].astype(F32) + u1[r, :].astype(F32) + v1[r, :].astype(F32)
            ).astype(BF16)
            push(g, exchange(g, part, 9, q1.at[r, small(2)], t2.at[r], minor(1)))
            push(g, exchange(g, part, 10, q1.at[r, small(-1)], v2.at[r], minor(-1)))

    def c7(g):
        for part in range(2):
            minor, _, _, _, small, r = ring(part, g, R2, first2)
            exchange(g, part, 9, t2.at[r], t2.at[r], minor(1)).wait_recv()
            s2[r, :] = (t2[r, :].astype(F32) + q1[r, small(1)].astype(F32)).astype(BF16)
            push(g, exchange(g, part, 11, s2.at[r], u2.at[r], minor(1)))

    def back(r):
        dz = distance(r // 2)
        zt = lax.rem(z + dz, NZ)
        ct = lax.rem(c + r, 2)
        lo = pl.multiple_of(r * CAP, CAP)
        return remote(
            fin.at[pl.ds(lo, CAP), :], ret.at[me_sp], rsend, rrecv, (zt, ct, y, x)
        )

    def c8(g):
        for part in range(2):
            minor, _, _, _, small, r = ring(part, g, R2, first2)
            exchange(g, part, 10, v2.at[r], v2.at[r], minor(1)).wait_recv()
            exchange(g, part, 11, u2.at[r], u2.at[r], minor(1)).wait_recv()
            fin[r, :] = (
                q1[r, small(0)].astype(F32) + u2[r, :].astype(F32) + v2[r, :].astype(F32)
            ).astype(BF16)
            for i in range(CHUNKS):
                k = (g * 2 + part) * CHUNKS + i

                @pl.when(k != r_self)
                def _(k=k):
                    back(k).start()

    pipeline(
        (
            (8, c8),
            (7, c7),
            (6, c6),
            (5, c5),
            (3, b3),
            (2, b2),
            (1, b1),
            (0, first_stage),
            (4, expert_stage),
        ),
        G2,
    )
    ret[me_sp] = fin[r_self * CAP : (r_self + 1) * CAP, :]

    bdrain()
    for part in range(2):
        minor, major, _, wide, small, r = ring(part, 0, R2, first2)
        for kind in (6, 7, 8):
            exchange(0, part, kind, t1.at[r], t1.at[r], major(1)).wait_send()
        for kind in (9, 10, 11):
            exchange(0, part, kind, t2.at[r], t2.at[r], minor(1)).wait_send()
    others = ret.at[pl.ds(0, EXPERTS - 1)]
    pltpu.make_async_copy(others, others, dsend).wait()
    pltpu.make_async_copy(others, others, rrecv).wait()
    pltpu.make_async_copy(others, others, rsend).wait()

    back_rows = ret[...].reshape(SLOTS, LANES)
    total = jnp.zeros((ROWS, LANES), F32)
    for k in range(2):
        picked = jnp.dot(pick[k], back_rows, preferred_element_type=F32)
        total = total + picked * to_column(rw[k : k + 1, :])
    out[...] = (strm[...].astype(F32) + total).astype(BF16)


def per_device(
    residual_in,
    conv_value,
    conv_gate,
    doc_ids,
    conv_kernel,
    ln_gain,
    out_weight,
    norm_gain,
    routes,
    route_weight,
    gate_w,
    up_w,
    down_w,
):
    vmem = pl.BlockSpec(memory_space=pltpu.VMEM)
    hbm = pl.BlockSpec(memory_space=pl.ANY)
    dma = pltpu.SemaphoreType.DMA
    hidden = gate_w.shape[2]
    return pl.pallas_call(
        kernel,
        out_shape=jax.ShapeDtypeStruct((ROWS, LANES), BF16),
        in_specs=[vmem] * 9 + [hbm] * 4,
        out_specs=vmem,
        scratch_shapes=[
            pltpu.VMEM((FULL, LANES), BF16),
            pltpu.VMEM((FULL, hidden), BF16),
            pltpu.VMEM((FULL, hidden), BF16),
            pltpu.VMEM((hidden, FULL), BF16),
            pltpu.VMEM((HALO + ROWS, LANES), F32),
            pltpu.VMEM((HALO + ROWS, LANES), F32),
            pltpu.VMEM((HALO, LANES), BF16),
            pltpu.VMEM((HALO, LANES), F32),
            pltpu.VMEM((HALO, LANES), BF16),
            pltpu.VMEM((HALO, LANES), F32),
            pltpu.VMEM((ROWS, LANES), F32),
            pltpu.VMEM((NTP, 8, ROWS), F32),
            pltpu.VMEM((8, FULL), F32),
            pltpu.VMEM((ROWS, LANES), F32),
            pltpu.VMEM((ROWS, FULL), BF16),
            pltpu.VMEM((ROWS, FULL), BF16),
            pltpu.VMEM((ROWS, LANES), BF16),
            pltpu.VMEM((2, ROWS, SLOTS), BF16),
            pltpu.VMEM((EXPERTS, CAP, LANES), BF16),
            pltpu.VMEM((SLOTS, FULL), BF16),
            pltpu.VMEM((2 * R2, FULL), BF16),
            pltpu.VMEM((2 * R2, hidden), BF16),
            pltpu.VMEM((SLOTS, FULL), BF16),
            pltpu.VMEM((SLOTS, WIDE), BF16),
            pltpu.VMEM((SLOTS, WIDE), BF16),
            pltpu.VMEM((SLOTS, WIDE), BF16),
            pltpu.VMEM((SLOTS, WIDE), BF16),
            pltpu.VMEM((SLOTS, WIDE), BF16),
            pltpu.VMEM((SLOTS, LANES), BF16),
            pltpu.VMEM((SLOTS, LANES), BF16),
            pltpu.VMEM((SLOTS, LANES), BF16),
            pltpu.VMEM((SLOTS, LANES), BF16),
            pltpu.VMEM((SLOTS, LANES), BF16),
            pltpu.VMEM((EXPERTS, CAP, LANES), BF16),
            dma((4,)),
            dma((2,)),
            dma((2,)),
            dma((NTP,)),
            dma((NTP,)),
            dma((2, 6)),
            dma((G1, 2, 6)),
            dma((2, 12)),
            dma((G2, 2, 12)),
            dma(()),
            dma((2 * G2,)),
            dma(()),
            dma(()),
        ],
        compiler_params=pltpu.CompilerParams(
            collective_id=0, has_side_effects=True, vmem_limit_bytes=60 * 1024 * 1024
        ),
        name="layer",
    )(
        conv_value,
        conv_gate,
        doc_ids.reshape(1, ROWS),
        conv_kernel,
        ln_gain.reshape(1, LANES),
        residual_in,
        routes.T,
        route_weight.T,
        norm_gain.reshape(1, LANES),
        out_weight,
        gate_w,
        up_w,
        down_w,
    )


def solution(mesh):
    split = Mesh(mesh.devices.reshape(NZ, 2, RING, RING), AXES)
    in_specs = (
        P(SP, TP),
        P(SP, TP),
        P(SP, TP),
        P(SP),
        P(None, TP),
        P(TP),
        P(None, TP),
        P(TP),
        P(SP, None),
        P(SP, None),
        P(SP, None, TP),
        P(SP, None, TP),
        P(SP, TP, None),
    )
    return jax.shard_map(
        per_device, mesh=split, in_specs=in_specs, out_specs=P(SP, TP), check_vma=False
    )
```

time: 284 us -> 120 us (0.42)
  blocking collectives: 182 us -> 0 us
  Pallas kernels: 0 us -> 118 us
  waiting for transfers between devices: 32 us -> 0 us
  local copies, waits for them, and re-layouts: 25.6 us -> 1.47 us
  starting transfers between devices: 17.7 us -> 0 us
  other arithmetic: 14.6 us -> 0 us
  matrix products: 11.5 us -> 0 us
    all_to_all x3 -> x0, blocking collectives: 151 us -> none  [the longest x1 53.1 us: sum_at_owner(): pieces = lax.all_to_all(in_blocks(x, dim, peers), axis, 0, 0, tiled=True)]
    pallas_call x0 -> x1, Pallas kernels: none -> 118 us  [per_device(): pl.pallas_call(kernel, out_shape=jax.ShapeDtypeStruct((ROWS, LANES), BF16...]
    all_to_all x2 -> x0, waiting for transfers between devices: 32 us -> none  [the longest x1 21.7 us: per_device(): lax.all_to_all(summed, 'sp', split_axis=0, concat_axis=0, tiled=True)]
    psum x4 -> x0, blocking collectives: 30.3 us -> none  [over_axes(): x = lax.psum(x, axis)]
    dot_general x3 -> x0, matrix products: 11.5 us -> none  [the longest x1 8.8 us: per_device(): jnp.dot(hidden, down_w[0], preferred_element_type=jnp.float32)]
    all_to_all x2 -> x0, starting transfers between devices: 10.9 us -> none  [the longest x1 7.24 us: per_device(): lax.all_to_all(summed, 'sp', split_axis=0, concat_axis=0, tiled=True)]
    reduce_sum x4 -> x0, other arithmetic: 6.95 us -> none  [the longest x1 3.53 us: sum_at_owner(): return jnp.sum(pieces.astype(jnp.float32), axis=0)]
    ppermute x2 -> x0, starting transfers between devices: 6.83 us -> none  [from_behind(): return lax.ppermute(x, axis, pairs)]
  transfers between devices with their start and end apart: 4 -> 0, of which waited for: 2 -> 0; matrix products, arithmetic and copies ran while one was open for 5% -> 0% of each run, Pallas kernels for 0% -> 0%
where the time goes in v1:
time: 120 us
  Pallas kernels  118 us (98%)
  local copies, waits for them, and re-layouts  1.47 us (1%)
    pallas_call x1, Pallas kernels, per_device(): pl.pallas_call(kernel, out_shape=jax.ShapeDtypeStruct((ROWS, LANES), BF16...  118 us

profile of v1, /device:TPU:1, one launch (start us, length us, event | category | flops | bytes accessed | tf_op | source)
XLA Modules:
  0.0 119.8 jit_solution(7537160312453240491)
XLA Ops:
  0.0 118.3 %layer.1 = bf16[256,128]{1,0:T(8,128)(2,1)} custom-call(bf16[256,128]{1,0:T(8,128)(2,1)} %cv.1, bf16[256,128]{1,0:T(8,128)(2,1)} %cg.1, s32[1,256]{1,0:T(1,128)} %bitcast.7, bf16[31,128]{1,0:T(8,128)(2,1)} %ck.1, bf16[1,128]{1,0:T(2,128)(2,1)} %bitcast.8, bf16[256,128]{1,0:T(8,128)(2,1)} %res.1, s32[2,256]{1,0:T(2,128)} %bitcast.5, f32[2,256]{1,0:T(2,128)} %bitcast.6, ...), custom_call_target="tpu_custom_call" | custom-call | tf_op jit(solution)/shard_map/layer/pallas_call | solution.py:621
  118.3 1.5 %copy.15 = bf16[256,128]{1,0:T(8,128)(2,1)} copy(bf16[256,128]{1,0:T(8,128)(2,1)} %layer.1) | data formatting | bytes 131072

commit v2 on v1

--- a/solution.py
+++ b/solution.py
@@ -33,7 +33,14 @@
 R1 = ROWS // G1 // 2
 R2 = SLOTS // G2 // 2
 CHUNKS = R2 // CAP
-ZFIRST = 4
+REACH = (0, 1, 15, 2, 12, 5, 11, 6, 10, 7, 9, 8, 14, 3, 13, 4)
+ORDER = (
+    0, 1, 10, 11, 20, 21, 100, 101, 30, 31, 110, 111,
+    120, 121, 201, 200, 131, 130, 210, 211, 221, 220, 300, 230,
+    231, 310, 320, 400, 401, 330, 410, 411, 420, 421, 500, 501,
+    430, 431, 510, 511, 520, 521, 600, 601, 530, 531, 610, 611,
+    620, 621, 630, 631,
+)
 
 
 def remote(src, dst, send, recv, dev):
@@ -45,12 +52,6 @@
         device_id=dev,
         device_id_type=MESH,
     )
-
-
-def distance(i):
-    k = lax.rem(i + ZFIRST, NZ)
-    half = (k + 1) // 2
-    return jnp.where(lax.rem(k, 2) == 1, half, NZ - half)
 
 
 def to_column(row):
@@ -123,6 +124,7 @@
     drecv,
     rsend,
     rrecv,
+    ready,
 ):
     z = lax.axis_index("z")
     c = lax.axis_index("core")
@@ -146,20 +148,20 @@
         other = lax.rem(me_tp + k, NTP)
         return (z, c, other // RING, lax.rem(other, RING))
 
-    def sp_peer(k):
-        other = lax.rem(me_sp + k, 2 * NZ)
-        return (other // 2, lax.rem(other, 2), y, x)
-
-    def greet_tp(k, carry):
-        pl.semaphore_signal(barrier, inc=1, device_id=tp_peer(k), device_id_type=MESH)
+    def along(by, core):
+        return (lax.rem(z + by + NZ, NZ), core, y, x)
+
+    def tell(sem, dev):
+        pl.semaphore_signal(sem, inc=1, device_id=dev, device_id_type=MESH)
+
+    def greet(k, carry):
+        tell(barrier, tp_peer(k))
         return carry
 
-    def greet_sp(k, carry):
-        pl.semaphore_signal(barrier, inc=1, device_id=sp_peer(k), device_id_type=MESH)
-        return carry
-
-    lax.fori_loop(1, 2 * NZ, greet_sp, 0)
-    lax.fori_loop(1, NTP, greet_tp, 0)
+    beside = along(2 * c - 1, 1 - c)
+    for dev in (along(1, c), along(-1, c), along(0, 1 - c), beside):
+        tell(barrier, dev)
+    lax.fori_loop(1, NTP, greet, 0)
 
     gate = cg[...].astype(F32)
     gated = (cv[...].astype(F32) * (1.0 / (1.0 + jnp.exp(-gate)))).astype(BF16)
@@ -183,9 +185,19 @@
     for first in range(HALO, ROWS, 32):
         conv_rows(first, 32)
 
-    pl.semaphore_wait(barrier, NTP - 1 + 2 * NZ - 1)
-
-    after = sp_peer(1)
+    pl.semaphore_wait(barrier, NTP - 1 + 4)
+
+    def spread_word(i):
+        if i > 0:
+            pl.semaphore_wait(ready.at[i - 1], 1 if i == 1 else 2)
+        if i == 0:
+            tell(ready.at[0], along(0, 1 - c))
+        elif i < 4:
+            for by in (1 << (i - 1), -(1 << (i - 1))):
+                tell(ready.at[i], along(by, c))
+
+    spread_word(0)
+    after = along(c, 1 - c)
     halo_g = remote(hg_out, hg_in, hsend.at[0], hrecv.at[0], after)
     halo_d = remote(hd_out, hd_in, hsend.at[1], hrecv.at[1], after)
     halo_g.start()
@@ -213,6 +225,7 @@
 
     halo_g.wait()
     halo_d.wait()
+    spread_word(1)
     first_block = me_sp == 0
     ext[:HALO, :] = hg_in[...].astype(F32)
     docx[:HALO, :] = jnp.where(first_block, -1.0, hd_in[...])
@@ -241,7 +254,7 @@
 
     def ring(part, g, rows, first):
         mm, mj = (x, y) if part == 0 else (y, x)
-        step = 1 - 2 * (g % 2) if isinstance(g, int) else 1 - 2 * lax.rem(g, 2)
+        step = 1 - 2 * (g % 2)
 
         def at(base, by):
             return lax.rem(base + by * step + 2 * RING, RING)
@@ -263,90 +276,58 @@
         def small(by):
             return pl.ds(pl.multiple_of(at(mm, by) * LANES, LANES), LANES)
 
-        lo = pl.multiple_of(first(g, part), rows)
-        return minor, major, block, wide, small, pl.ds(lo, rows)
+        return minor, major, block, wide, small, pl.ds(first(g, part), rows)
+
+    flying = {}
+
+    def push(ssem, part, kind, d):
+        key = (id(ssem), part, kind)
+        if key in flying:
+            flying[key].wait_send()
+        d.start()
+        flying[key] = d
 
     def make_gather(buf, rows, first, ssem, rsem):
         def move(g, part, kind, cols, dev):
-            r = pl.ds(pl.multiple_of(first(g, part), rows), rows)
-            ref = buf.at[r, cols]
+            ref = buf.at[pl.ds(first(g, part), rows), cols]
             return remote(ref, ref, ssem.at[part, kind], rsem.at[g, part, kind], dev)
 
-        def send(g, part, kind, cols, dev):
-            d = move(g, part, kind, cols, dev)
-
-            if isinstance(g, int):
-                if g > 0:
-                    d.wait_send()
-            else:
-                pl.when(g > 0)(d.wait_send)
-            d.start()
-
-        def s0(g):
-            for part in range(2):
-                minor, _, block, _, _, _ = ring(part, g, rows, first)
-                send(g, part, 0, block(0), minor(1))
-                send(g, part, 1, block(0), minor(-1))
-
-        def s1(g):
-            for part in range(2):
-                minor, _, block, _, _, _ = ring(part, g, rows, first)
-                move(g, part, 0, block(-1), minor(1)).wait_recv()
-                send(g, part, 2, block(-1), minor(1))
-
-        def s2(g):
-            for part in range(2):
-                minor, major, block, wide, _, _ = ring(part, g, rows, first)
-                move(g, part, 1, block(1), minor(1)).wait_recv()
-                move(g, part, 2, block(2), minor(1)).wait_recv()
-                send(g, part, 3, wide(0), major(1))
-                send(g, part, 4, wide(0), major(-1))
-
-        def s3(g):
-            for part in range(2):
-                _, major, _, wide, _, _ = ring(part, g, rows, first)
-                move(g, part, 3, wide(-1), major(1)).wait_recv()
-                send(g, part, 5, wide(-1), major(1))
-
-        def s4(g):
-            for part in range(2):
-                _, major, _, wide, _, _ = ring(part, g, rows, first)
-                move(g, part, 4, wide(1), major(1)).wait_recv()
-                move(g, part, 5, wide(2), major(1)).wait_recv()
-
-        def drain():
-            for part in range(2):
-                minor, major, block, wide, _, _ = ring(part, 0, rows, first)
-                for kind in range(3):
-                    move(0, part, kind, block(0), minor(1)).wait_send()
-                for kind in range(3, 6):
-                    move(0, part, kind, wide(0), major(1)).wait_send()
-
-        return s0, s1, s2, s3, s4, drain
-
-    def pipeline(stages, groups):
-        last = max(d for d, _ in stages)
-
-        def step(t, carry):
-            for delay, stage in stages:
-                g = t - delay
-
-                @pl.when((g >= 0) & (g < groups))
-                def _(stage=stage, g=g):
-                    stage(g)
-
-            return carry
-
-        lax.fori_loop(0, groups + last, step, 0)
+        def own(g, part):
+            minor, _, block, _, _, _ = ring(part, g, rows, first)
+            for kind, by in enumerate((1, -1, 2)):
+                push(ssem, part, kind, move(g, part, kind, block(0), minor(by)))
+
+        def sets(g, part):
+            minor, major, block, wide, _, _ = ring(part, g, rows, first)
+            for kind, by in enumerate((-1, 1, 2)):
+                move(g, part, kind, block(by), minor(1)).wait_recv()
+            push(ssem, part, 3, move(g, part, 3, wide(0), major(1)))
+            push(ssem, part, 4, move(g, part, 4, wide(0), major(-1)))
+
+        def relay(g, part):
+            _, major, _, wide, _, _ = ring(part, g, rows, first)
+            move(g, part, 3, wide(-1), major(1)).wait_recv()
+            push(ssem, part, 5, move(g, part, 5, wide(-1), major(1)))
+
+        def landed(g, part):
+            _, major, _, wide, _, _ = ring(part, g, rows, first)
+            move(g, part, 4, wide(1), major(1)).wait_recv()
+            move(g, part, 5, wide(2), major(1)).wait_recv()
+
+        return own, sets, relay, landed
 
     def first1(g, part):
         return g * 2 * R1 + part * R1
 
-    a0, a1, a2, a3, a4, adrain = make_gather(xg, R1, first1, ssem1, rsem1)
-    for g in range(G1):
-        a0(g)
+    own1, sets1, relay1, landed1 = make_gather(xg, R1, first1, ssem1, rsem1)
+    moves1 = [(g, part) for g in range(G1) for part in range(2)]
+    for g, part in moves1:
+        own1(g, part)
     lax.fori_loop(1, NTP, send_stat, 0)
-    pipeline(((4, a4), (3, a3), (2, a2), (1, a1)), G1)
+    spread_word(2)
+    for g, part in moves1:
+        sets1(g, part)
+    spread_word(3)
 
     def wait_stat(k, carry):
         d = remote(stat.at[me_tp], stat.at[me_tp], stsend.at[k], strecv.at[k], tp_peer(k))
@@ -355,7 +336,8 @@
         return carry
 
     lax.fori_loop(1, NTP, wait_stat, 0)
-    adrain()
+    for g, part in moves1[:2]:
+        relay1(g, part)
 
     means = [stat[j, 0:1, :] for j in range(NTP)]
     mean = sum(means) * (1.0 / NTP)
@@ -372,11 +354,11 @@
             [stat[j, 2:3, :LANES], stat[j, 2:3, LANES:], jnp.zeros((6, LANES), F32)], axis=0
         )
 
-    for part in range(2):
-
-        def normalise(i, carry, part=part):
-            g = i // (R1 // 16)
-            lo = pl.multiple_of(first1(g, part) + lax.rem(i, R1 // 16) * 16, 16)
+    def normalise(g, part):
+        landed1(g, part)
+
+        def some(i, carry):
+            lo = pl.multiple_of(first1(g, part) + i * 16, 16)
             cs = colstat[pl.ds(lo, 16), :]
             rs = cs[:, NTP : NTP + 1]
             for pos in range(NTP):
@@ -387,7 +369,13 @@
                 act[pl.ds(lo, 16), j * LANES : (j + 1) * LANES] = v.astype(BF16)
             return carry
 
-        lax.fori_loop(0, G1 * R1 // 16, normalise, 0)
+        lax.fori_loop(0, R1 // 16, some, 0)
+
+    for i, (g, part) in enumerate(moves1):
+        if i + 2 < len(moves1):
+            relay1(*moves1[i + 2])
+        normalise(g, part)
+    spread_word(4)
 
     weights[0].wait()
     projected = jnp.dot(act[...], ow[...], preferred_element_type=F32).astype(BF16)
@@ -401,65 +389,30 @@
         .reshape(EXPERTS, CAP, LANES)
     )
 
-    pos_a = pl.multiple_of((y * RING + x) * LANES, LANES)
-    pos_b = pl.multiple_of((x * RING + y) * LANES, LANES)
-
-    def own_pos(r):
-        return pl.multiple_of(jnp.where(lax.rem(r // CHUNKS, 2) == 0, pos_a, pos_b), LANES)
-
-    r_self = ((NZ - ZFIRST) % NZ) * 2
-    g_self, part_self = r_self // (2 * CHUNKS), (r_self // CHUNKS) % 2
-
-    def dispatch(r, turn):
-        dz = distance(r // 2)
-        zt = lax.rem(z - dz + NZ, NZ)
-        ct = lax.rem(c + r, 2)
-        lo = pl.multiple_of(r * CAP, CAP)
-        return remote(
-            dsp.at[zt * 2 + ct],
-            x2g.at[pl.ds(lo, CAP), pl.ds(own_pos(r), LANES)],
-            dsend,
-            drecv.at[r // CHUNKS],
-            (zt, ct, y, x),
-        )
-
-    def send_dispatch(r, carry):
-        @pl.when(r != r_self)
-        def _():
-            dispatch(r, 0).start()
-
-        return carry
-
-    lax.fori_loop(0, EXPERTS, send_dispatch, 0)
-    x2g[r_self * CAP : (r_self + 1) * CAP, pl.ds(own_pos(jnp.int32(r_self)), LANES)] = dsp[me_sp]
+    own_pos = [
+        pl.multiple_of((y * RING + x) * LANES, LANES),
+        pl.multiple_of((x * RING + y) * LANES, LANES),
+    ]
+
+    def here(r):
+        part = (r // CHUNKS) % 2
+        return x2g.at[pl.ds(r * CAP, CAP), pl.ds(own_pos[part], LANES)]
+
+    for r in range(1, EXPERTS):
+        dev = along(-REACH[r // 2], lax.rem(c + r, 2))
+        remote(dsp.at[dev[0] * 2 + dev[1]], here(r), dsend, drecv.at[r // CHUNKS], dev).start()
+    x2g[:CAP, pl.ds(own_pos[0], LANES)] = dsp[me_sp]
 
     def first2(g, part):
         return g * 2 * R2 + part * R2
 
-    b0, b1, b2, b3, b4, bdrain = make_gather(x2g, R2, first2, ssem2, rsem2)
-
-    def arrivals(g):
-        for part in range(2):
-            pos = pos_a if part == 0 else pos_b
-            lo = pl.multiple_of(first2(g, part), R2)
-            sem = drecv.at[g * 2 + part]
-            full = x2g.at[pl.ds(lo, R2), pl.ds(pos, LANES)]
-            less = x2g.at[pl.ds(lo, R2 - CAP), pl.ds(pos, LANES)]
-            if part == part_self:
-
-                @pl.when(g == g_self)
-                def _():
-                    pltpu.make_async_copy(less, less, sem).wait()
-
-                @pl.when(g != g_self)
-                def _():
-                    pltpu.make_async_copy(full, full, sem).wait()
-            else:
-                pltpu.make_async_copy(full, full, sem).wait()
-
-    def first_stage(g):
-        arrivals(g)
-        b0(g)
+    own2, sets2, relay2, landed2 = make_gather(x2g, R2, first2, ssem2, rsem2)
+
+    def arrived(g, part):
+        rows = R2 - CAP if g + part == 0 else R2
+        ref = x2g.at[pl.ds(first2(g, part), rows), pl.ds(own_pos[part], LANES)]
+        pltpu.make_async_copy(ref, ref, drecv.at[g * 2 + part]).wait()
+        own2(g, part)
 
     for w in weights[1:]:
         w.wait()
@@ -467,16 +420,10 @@
     def exchange(g, part, kind, src, dst, dev):
         return remote(src, dst, ssem2.at[part, kind], rsem2.at[g, part, kind], dev)
 
-    def push(g, d):
-        @pl.when(g > 0)
-        def _():
-            d.wait_send()
-
-        d.start()
-
-    def expert_stage(g):
-        b4(g)
-        base = pl.multiple_of(g * 2 * R2, 2 * R2)
+    def expert_stage(g, _):
+        landed2(g, 0)
+        landed2(g, 1)
+        base = g * 2 * R2
         for part in range(2):
 
             def norm_rows(i, carry, part=part):
@@ -511,81 +458,50 @@
                 ]
         for part in range(2):
             _, major, _, wide, _, r = ring(part, g, R2, first2)
-            push(g, exchange(g, part, 6, part_sum.at[r, wide(2)], t1.at[r], major(1)))
-            push(g, exchange(g, part, 7, part_sum.at[r, wide(-1)], v1.at[r], major(-1)))
-
-    def c5(g):
-        for part in range(2):
-            _, major, _, wide, _, r = ring(part, g, R2, first2)
-            exchange(g, part, 6, t1.at[r], t1.at[r], major(1)).wait_recv()
-            s1[r, :] = (t1[r, :].astype(F32) + part_sum[r, wide(1)].astype(F32)).astype(BF16)
-            push(g, exchange(g, part, 8, s1.at[r], u1.at[r], major(1)))
-
-    def c6(g):
-        for part in range(2):
-            minor, major, _, wide, small, r = ring(part, g, R2, first2)
-            exchange(g, part, 7, v1.at[r], v1.at[r], major(1)).wait_recv()
-            exchange(g, part, 8, u1.at[r], u1.at[r], major(1)).wait_recv()
-            q1[r, :] = (
-                part_sum[r, wide(0)].astype(F32) + u1[r, :].astype(F32) + v1[r, :].astype(F32)
-            ).astype(BF16)
-            push(g, exchange(g, part, 9, q1.at[r, small(2)], t2.at[r], minor(1)))
-            push(g, exchange(g, part, 10, q1.at[r, small(-1)], v2.at[r], minor(-1)))
-
-    def c7(g):
-        for part in range(2):
-            minor, _, _, _, small, r = ring(part, g, R2, first2)
-            exchange(g, part, 9, t2.at[r], t2.at[r], minor(1)).wait_recv()
-            s2[r, :] = (t2[r, :].astype(F32) + q1[r, small(1)].astype(F32)).astype(BF16)
-            push(g, exchange(g, part, 11, s2.at[r], u2.at[r], minor(1)))
-
-    def back(r):
-        dz = distance(r // 2)
-        zt = lax.rem(z + dz, NZ)
-        ct = lax.rem(c + r, 2)
-        lo = pl.multiple_of(r * CAP, CAP)
-        return remote(
-            fin.at[pl.ds(lo, CAP), :], ret.at[me_sp], rsend, rrecv, (zt, ct, y, x)
-        )
-
-    def c8(g):
-        for part in range(2):
-            minor, _, _, _, small, r = ring(part, g, R2, first2)
-            exchange(g, part, 10, v2.at[r], v2.at[r], minor(1)).wait_recv()
-            exchange(g, part, 11, u2.at[r], u2.at[r], minor(1)).wait_recv()
-            fin[r, :] = (
-                q1[r, small(0)].astype(F32) + u2[r, :].astype(F32) + v2[r, :].astype(F32)
-            ).astype(BF16)
-            for i in range(CHUNKS):
-                k = (g * 2 + part) * CHUNKS + i
-
-                @pl.when(k != r_self)
-                def _(k=k):
-                    back(k).start()
-
-    pipeline(
-        (
-            (8, c8),
-            (7, c7),
-            (6, c6),
-            (5, c5),
-            (3, b3),
-            (2, b2),
-            (1, b1),
-            (0, first_stage),
-            (4, expert_stage),
-        ),
-        G2,
-    )
-    ret[me_sp] = fin[r_self * CAP : (r_self + 1) * CAP, :]
-
-    bdrain()
-    for part in range(2):
-        minor, major, _, wide, small, r = ring(part, 0, R2, first2)
-        for kind in (6, 7, 8):
-            exchange(0, part, kind, t1.at[r], t1.at[r], major(1)).wait_send()
-        for kind in (9, 10, 11):
-            exchange(0, part, kind, t2.at[r], t2.at[r], minor(1)).wait_send()
+            send(g, part, 6, part_sum.at[r, wide(2)], t1.at[r], major(1))
+            send(g, part, 7, part_sum.at[r, wide(-1)], v1.at[r], major(-1))
+
+    def send(g, part, kind, src, dst, dev):
+        push(ssem2, part, kind, exchange(g, part, kind, src, dst, dev))
+
+    def pass_on(g, part):
+        _, major, _, wide, _, r = ring(part, g, R2, first2)
+        exchange(g, part, 6, t1.at[r], t1.at[r], major(1)).wait_recv()
+        s1[r, :] = (t1[r, :].astype(F32) + part_sum[r, wide(1)].astype(F32)).astype(BF16)
+        send(g, part, 8, s1.at[r], u1.at[r], major(1))
+
+    def ring_sum(g, part):
+        minor, major, _, wide, small, r = ring(part, g, R2, first2)
+        exchange(g, part, 7, v1.at[r], v1.at[r], major(1)).wait_recv()
+        exchange(g, part, 8, u1.at[r], u1.at[r], major(1)).wait_recv()
+        q1[r, :] = (
+            part_sum[r, wide(0)].astype(F32) + u1[r, :].astype(F32) + v1[r, :].astype(F32)
+        ).astype(BF16)
+        for kind, by, dst in ((9, 1, t2), (10, -1, v2), (11, 2, u2)):
+            send(g, part, kind, q1.at[r, small(by)], dst.at[r], minor(by))
+
+    def last_sum(g, part):
+        minor, _, _, _, small, r = ring(part, g, R2, first2)
+        total = q1[r, small(0)].astype(F32)
+        for kind, dst in ((9, t2), (10, v2), (11, u2)):
+            exchange(g, part, kind, dst.at[r], dst.at[r], minor(1)).wait_recv()
+        fin[r, :] = (
+            total + t2[r, :].astype(F32) + v2[r, :].astype(F32) + u2[r, :].astype(F32)
+        ).astype(BF16)
+        for i in range(CHUNKS):
+            k = (g * 2 + part) * CHUNKS + i
+            if k > 0:
+                dev = along(REACH[k // 2], lax.rem(c + k, 2))
+                src = fin.at[pl.ds(k * CAP, CAP), :]
+                remote(src, ret.at[me_sp], rsend, rrecv, dev).start()
+
+    moves2 = (arrived, sets2, relay2, expert_stage, pass_on, ring_sum, last_sum)
+    for code in ORDER:
+        moves2[code // 100](code // 10 % 10, code % 10)
+    ret[me_sp] = fin[:CAP, :]
+
+    for d in flying.values():
+        d.wait_send()
     others = ret.at[pl.ds(0, EXPERTS - 1)]
     pltpu.make_async_copy(others, others, dsend).wait()
     pltpu.make_async_copy(others, others, rrecv).wait()
@@ -671,6 +587,7 @@
             dma((2 * G2,)),
             dma(()),
             dma(()),
+            pltpu.SemaphoreType.REGULAR((4,)),
         ],
         compiler_params=pltpu.CompilerParams(
             collective_id=0, has_side_effects=True, vmem_limit_bytes=60 * 1024 * 1024

time: 120 us -> 110 us (0.917)
  Pallas kernels: 118 us -> 109 us
    pallas_call x1, Pallas kernels: 118 us -> 109 us  [per_device(): pl.pallas_call(kernel, out_shape=jax.ShapeDtypeStruct((ROWS, LANES), BF16...]
where the time goes in v2:
time: 110 us
  Pallas kernels  109 us (99%)
  local copies, waits for them, and re-layouts  1.47 us (1%)
    pallas_call x1, Pallas kernels, per_device(): pl.pallas_call(kernel, out_shape=jax.ShapeDtypeStruct((ROWS, LANES), BF16...  109 us

profile of v2, /device:TPU:1, one launch (start us, length us, event | category | flops | bytes accessed | tf_op | source)
XLA Modules:
  0.0 110.1 jit_solution(8146456048438670831)
XLA Ops:
  0.0 108.6 %layer.1 = bf16[256,128]{1,0:T(8,128)(2,1)} custom-call(bf16[256,128]{1,0:T(8,128)(2,1)} %cv.1, bf16[256,128]{1,0:T(8,128)(2,1)} %cg.1, s32[1,256]{1,0:T(1,128)} %bitcast.7, bf16[31,128]{1,0:T(8,128)(2,1)} %ck.1, bf16[1,128]{1,0:T(2,128)(2,1)} %bitcast.8, bf16[256,128]{1,0:T(8,128)(2,1)} %res.1, s32[2,256]{1,0:T(2,128)} %bitcast.5, f32[2,256]{1,0:T(2,128)} %bitcast.6, ...), custom_call_target="tpu_custom_call" | custom-call | tf_op jit(solution)/shard_map/layer/pallas_call | solution.py:537
  108.6 1.5 %copy.15 = bf16[256,128]{1,0:T(8,128)(2,1)} copy(bf16[256,128]{1,0:T(8,128)(2,1)} %layer.1) | data formatting | bytes 131072

commit v3 on v2

--- a/solution.py
+++ b/solution.py
@@ -29,17 +29,18 @@
 SLOTS = EXPERTS * CAP
 NZ = 16
 G1 = 2
-G2 = 4
 R1 = ROWS // G1 // 2
-R2 = SLOTS // G2 // 2
-CHUNKS = R2 // CAP
+SIZES = (2, 4, 4, 4, 2)
+G2 = len(SIZES)
+BIG = 2 * max(SIZES) * CAP
 REACH = (0, 1, 15, 2, 12, 5, 11, 6, 10, 7, 9, 8, 14, 3, 13, 4)
 ORDER = (
-    0, 1, 10, 11, 20, 21, 100, 101, 30, 31, 110, 111,
-    120, 121, 201, 200, 131, 130, 210, 211, 221, 220, 300, 230,
-    231, 310, 320, 400, 401, 330, 410, 411, 420, 421, 500, 501,
-    430, 431, 510, 511, 520, 521, 600, 601, 530, 531, 610, 611,
-    620, 621, 630, 631,
+    0, 1, 10, 11, 100, 101, 20, 21, 110, 111, 200, 201,
+    30, 31, 120, 121, 210, 211, 300, 40, 41, 130, 131, 220,
+    221, 310, 140, 141, 230, 231, 400, 401, 320, 240, 241, 410,
+    411, 330, 500, 501, 420, 421, 340, 510, 511, 600, 601, 430,
+    431, 520, 521, 610, 611, 440, 441, 530, 531, 620, 621, 540,
+    541, 630, 631, 640, 641,
 )
 
 
@@ -58,20 +59,39 @@
     return jnp.transpose(jnp.broadcast_to(row, (LANES, row.shape[1])))
 
 
+def first_chunk(g, part):
+    return 2 * sum(SIZES[:g]) + part * SIZES[g]
+
+
+def first2(g, part):
+    return first_chunk(g, part) * CAP
+
+
+def rows2(g):
+    return SIZES[g] * CAP
+
+
+def rows1(g):
+    return R1
+
+
+PLACE = [(g, p) for g in range(G2) for p in range(2) for _ in range(SIZES[g])]
+
+
 def true_block(part, pos):
     return pos if part == 0 else (pos % RING) * RING + pos // RING
 
 
 def kernel(
-    cv,
-    cg,
-    doc,
-    ck,
-    lng,
-    res,
-    routes,
-    rw,
-    ng,
+    cv_hbm,
+    cg_hbm,
+    doc_hbm,
+    ck_hbm,
+    lng_hbm,
+    res_hbm,
+    routes_hbm,
+    rw_hbm,
+    ng_hbm,
     ow_hbm,
     gw_hbm,
     uw_hbm,
@@ -125,6 +145,16 @@
     rsend,
     rrecv,
     ready,
+    cv,
+    cg,
+    doc,
+    ck,
+    lng,
+    res,
+    routes,
+    rw,
+    ng,
+    isem,
 ):
     z = lax.axis_index("z")
     c = lax.axis_index("core")
@@ -139,7 +169,16 @@
             ((ow_hbm, ow), (gw_hbm.at[0], gw), (uw_hbm.at[0], uw), (dw_hbm.at[0], dw))
         )
     ]
-    for w in weights:
+    small_inputs = [
+        pltpu.make_async_copy(src, dst, isem.at[i])
+        for i, (src, dst) in enumerate(
+            zip(
+                (cv_hbm, cg_hbm, doc_hbm, ck_hbm, routes_hbm, lng_hbm, ng_hbm, rw_hbm, res_hbm),
+                (cv, cg, doc, ck, routes, lng, ng, rw, res),
+            )
+        )
+    ]
+    for w in small_inputs:
         w.start()
 
     barrier = pltpu.get_barrier_semaphore()
@@ -162,6 +201,11 @@
     for dev in (along(1, c), along(-1, c), along(0, 1 - c), beside):
         tell(barrier, dev)
     lax.fori_loop(1, NTP, greet, 0)
+
+    for w in weights:
+        w.start()
+    for w in small_inputs:
+        w.wait()
 
     gate = cg[...].astype(F32)
     gated = (cv[...].astype(F32) * (1.0 / (1.0 + jnp.exp(-gate)))).astype(BF16)
@@ -200,8 +244,11 @@
     after = along(c, 1 - c)
     halo_g = remote(hg_out, hg_in, hsend.at[0], hrecv.at[0], after)
     halo_d = remote(hd_out, hd_in, hsend.at[1], hrecv.at[1], after)
-    halo_g.start()
-    halo_d.start()
+
+    @pl.when(me_sp < 2 * NZ - 1)
+    def _():
+        halo_g.start()
+        halo_d.start()
 
     ids = routes[...]
     expert = lax.broadcasted_iota(jnp.int32, (EXPERTS, ROWS), 0)
@@ -223,11 +270,15 @@
                 (lane + float(b * LANES)) == col
             ).astype(BF16)
 
-    halo_g.wait()
-    halo_d.wait()
+    first_block = me_sp == 0
+
+    @pl.when(me_sp > 0)
+    def _():
+        halo_g.wait_recv()
+        halo_d.wait_recv()
+
     spread_word(1)
-    first_block = me_sp == 0
-    ext[:HALO, :] = hg_in[...].astype(F32)
+    ext[:HALO, :] = jnp.where(first_block, 0.0, hg_in[...].astype(F32))
     docx[:HALO, :] = jnp.where(first_block, -1.0, hd_in[...])
     conv_rows(0, HALO)
 
@@ -276,7 +327,7 @@
         def small(by):
             return pl.ds(pl.multiple_of(at(mm, by) * LANES, LANES), LANES)
 
-        return minor, major, block, wide, small, pl.ds(first(g, part), rows)
+        return minor, major, block, wide, small, pl.ds(first(g, part), rows(g))
 
     flying = {}
 
@@ -289,7 +340,7 @@
 
     def make_gather(buf, rows, first, ssem, rsem):
         def move(g, part, kind, cols, dev):
-            ref = buf.at[pl.ds(first(g, part), rows), cols]
+            ref = buf.at[pl.ds(first(g, part), rows(g)), cols]
             return remote(ref, ref, ssem.at[part, kind], rsem.at[g, part, kind], dev)
 
         def own(g, part):
@@ -319,7 +370,7 @@
     def first1(g, part):
         return g * 2 * R1 + part * R1
 
-    own1, sets1, relay1, landed1 = make_gather(xg, R1, first1, ssem1, rsem1)
+    own1, sets1, relay1, landed1 = make_gather(xg, rows1, first1, ssem1, rsem1)
     moves1 = [(g, part) for g in range(G1) for part in range(2)]
     for g, part in moves1:
         own1(g, part)
@@ -395,21 +446,18 @@
     ]
 
     def here(r):
-        part = (r // CHUNKS) % 2
+        part = PLACE[r][1]
         return x2g.at[pl.ds(r * CAP, CAP), pl.ds(own_pos[part], LANES)]
 
     for r in range(1, EXPERTS):
         dev = along(-REACH[r // 2], lax.rem(c + r, 2))
-        remote(dsp.at[dev[0] * 2 + dev[1]], here(r), dsend, drecv.at[r // CHUNKS], dev).start()
+        remote(dsp.at[dev[0] * 2 + dev[1]], here(r), dsend, drecv.at[PLACE[r][0] * 2 + PLACE[r][1]], dev).start()
     x2g[:CAP, pl.ds(own_pos[0], LANES)] = dsp[me_sp]
 
-    def first2(g, part):
-        return g * 2 * R2 + part * R2
-
-    own2, sets2, relay2, landed2 = make_gather(x2g, R2, first2, ssem2, rsem2)
+    own2, sets2, relay2, landed2 = make_gather(x2g, rows2, first2, ssem2, rsem2)
 
     def arrived(g, part):
-        rows = R2 - CAP if g + part == 0 else R2
+        rows = rows2(g) - CAP if g + part == 0 else rows2(g)
         ref = x2g.at[pl.ds(first2(g, part), rows), pl.ds(own_pos[part], LANES)]
         pltpu.make_async_copy(ref, ref, drecv.at[g * 2 + part]).wait()
         own2(g, part)
@@ -423,12 +471,12 @@
     def expert_stage(g, _):
         landed2(g, 0)
         landed2(g, 1)
-        base = g * 2 * R2
+        base, count = first2(g, 0), rows2(g)
         for part in range(2):
 
             def norm_rows(i, carry, part=part):
-                lo = pl.multiple_of(base + part * R2 + i * 16, 16)
-                to = pl.multiple_of(part * R2 + i * 16, 16)
+                lo = pl.multiple_of(base + part * count + i * 16, 16)
+                to = pl.multiple_of(part * count + i * 16, 16)
                 vals = [
                     x2g[pl.ds(lo, 16), pos * LANES : (pos + 1) * LANES].astype(F32)
                     for pos in range(NTP)
@@ -442,22 +490,23 @@
                     ).astype(BF16)
                 return carry
 
-            lax.fori_loop(0, R2 // 16, norm_rows, 0)
-        hg = jnp.dot(nrm[...], gw[...], preferred_element_type=F32)
-        hu = jnp.dot(nrm[...], uw[...], preferred_element_type=F32)
-        hid[...] = ((hg / (1.0 + jnp.exp(-hg))) * hu).astype(BF16)
+            lax.fori_loop(0, count // 16, norm_rows, 0)
+        both = pl.ds(0, 2 * count)
+        hg = jnp.dot(nrm[both, :], gw[...], preferred_element_type=F32)
+        hu = jnp.dot(nrm[both, :], uw[...], preferred_element_type=F32)
+        hid[both, :] = ((hg / (1.0 + jnp.exp(-hg))) * hu).astype(BF16)
         for q in range(RING):
             p = jnp.dot(
-                hid[...], dw[:, q * WIDE : (q + 1) * WIDE], preferred_element_type=F32
+                hid[both, :], dw[:, q * WIDE : (q + 1) * WIDE], preferred_element_type=F32
             ).astype(BF16)
-            part_sum[pl.ds(base, R2), q * WIDE : (q + 1) * WIDE] = p[:R2, :]
+            part_sum[pl.ds(base, count), q * WIDE : (q + 1) * WIDE] = p[:count, :]
             for i in range(RING):
                 at = (i * RING + q) * LANES
-                part_sum[pl.ds(base + R2, R2), at : at + LANES] = p[
-                    R2:, i * LANES : (i + 1) * LANES
+                part_sum[pl.ds(base + count, count), at : at + LANES] = p[
+                    count:, i * LANES : (i + 1) * LANES
                 ]
         for part in range(2):
-            _, major, _, wide, _, r = ring(part, g, R2, first2)
+            _, major, _, wide, _, r = ring(part, g, rows2, first2)
             send(g, part, 6, part_sum.at[r, wide(2)], t1.at[r], major(1))
             send(g, part, 7, part_sum.at[r, wide(-1)], v1.at[r], major(-1))
 
@@ -465,13 +514,13 @@
         push(ssem2, part, kind, exchange(g, part, kind, src, dst, dev))
 
     def pass_on(g, part):
-        _, major, _, wide, _, r = ring(part, g, R2, first2)
+        _, major, _, wide, _, r = ring(part, g, rows2, first2)
         exchange(g, part, 6, t1.at[r], t1.at[r], major(1)).wait_recv()
         s1[r, :] = (t1[r, :].astype(F32) + part_sum[r, wide(1)].astype(F32)).astype(BF16)
         send(g, part, 8, s1.at[r], u1.at[r], major(1))
 
     def ring_sum(g, part):
-        minor, major, _, wide, small, r = ring(part, g, R2, first2)
+        minor, major, _, wide, small, r = ring(part, g, rows2, first2)
         exchange(g, part, 7, v1.at[r], v1.at[r], major(1)).wait_recv()
         exchange(g, part, 8, u1.at[r], u1.at[r], major(1)).wait_recv()
         q1[r, :] = (
@@ -481,15 +530,15 @@
             send(g, part, kind, q1.at[r, small(by)], dst.at[r], minor(by))
 
     def last_sum(g, part):
-        minor, _, _, _, small, r = ring(part, g, R2, first2)
+        minor, _, _, _, small, r = ring(part, g, rows2, first2)
         total = q1[r, small(0)].astype(F32)
         for kind, dst in ((9, t2), (10, v2), (11, u2)):
             exchange(g, part, kind, dst.at[r], dst.at[r], minor(1)).wait_recv()
         fin[r, :] = (
             total + t2[r, :].astype(F32) + v2[r, :].astype(F32) + u2[r, :].astype(F32)
         ).astype(BF16)
-        for i in range(CHUNKS):
-            k = (g * 2 + part) * CHUNKS + i
+        for i in range(SIZES[g]):
+            k = first_chunk(g, part) + i
             if k > 0:
                 dev = along(REACH[k // 2], lax.rem(c + k, 2))
                 src = fin.at[pl.ds(k * CAP, CAP), :]
@@ -502,6 +551,12 @@
 
     for d in flying.values():
         d.wait_send()
+
+    @pl.when(me_sp < 2 * NZ - 1)
+    def _():
+        halo_g.wait_send()
+        halo_d.wait_send()
+
     others = ret.at[pl.ds(0, EXPERTS - 1)]
     pltpu.make_async_copy(others, others, dsend).wait()
     pltpu.make_async_copy(others, others, rrecv).wait()
@@ -537,7 +592,7 @@
     return pl.pallas_call(
         kernel,
         out_shape=jax.ShapeDtypeStruct((ROWS, LANES), BF16),
-        in_specs=[vmem] * 9 + [hbm] * 4,
+        in_specs=[hbm] * 13,
         out_specs=vmem,
         scratch_shapes=[
             pltpu.VMEM((FULL, LANES), BF16),
@@ -560,8 +615,8 @@
             pltpu.VMEM((2, ROWS, SLOTS), BF16),
             pltpu.VMEM((EXPERTS, CAP, LANES), BF16),
             pltpu.VMEM((SLOTS, FULL), BF16),
-            pltpu.VMEM((2 * R2, FULL), BF16),
-            pltpu.VMEM((2 * R2, hidden), BF16),
+            pltpu.VMEM((BIG, FULL), BF16),
+            pltpu.VMEM((BIG, hidden), BF16),
             pltpu.VMEM((SLOTS, FULL), BF16),
             pltpu.VMEM((SLOTS, WIDE), BF16),
             pltpu.VMEM((SLOTS, WIDE), BF16),
@@ -588,6 +643,16 @@
             dma(()),
             dma(()),
             pltpu.SemaphoreType.REGULAR((4,)),
+            pltpu.VMEM((ROWS, LANES), BF16),
+            pltpu.VMEM((ROWS, LANES), BF16),
+            pltpu.VMEM((1, ROWS), jnp.int32),
+            pltpu.VMEM((TAPS, LANES), BF16),
+            pltpu.VMEM((1, LANES), BF16),
+            pltpu.VMEM((ROWS, LANES), BF16),
+            pltpu.VMEM((2, ROWS), jnp.int32),
+            pltpu.VMEM((2, ROWS), F32),
+            pltpu.VMEM((1, LANES), BF16),
+            dma((9,)),
         ],
         compiler_params=pltpu.CompilerParams(
             collective_id=0, has_side_effects=True, vmem_limit_bytes=60 * 1024 * 1024

time: 110 us -> 105 us (0.955)
  Pallas kernels: 109 us -> 103 us
    pallas_call x1, Pallas kernels: 109 us -> 103 us  [per_device(): pl.pallas_call(kernel, out_shape=jax.ShapeDtypeStruct((ROWS, LANES), BF16...]
where the time goes in v3:
time: 105 us
  Pallas kernels  103 us (98%)
  local copies, waits for them, and re-layouts  1.47 us (1%)
    pallas_call x1, Pallas kernels, per_device(): pl.pallas_call(kernel, out_shape=jax.ShapeDtypeStruct((ROWS, LANES), BF16...  103 us

profile of v3, /device:TPU:1, one launch (start us, length us, event | category | flops | bytes accessed | tf_op | source)
XLA Modules:
  0.0 104.8 jit_solution(3958803701536975819)
XLA Ops:
  0.0 103.3 %layer.1 = bf16[256,128]{1,0:T(8,128)(2,1)} custom-call(bf16[256,128]{1,0:T(8,128)(2,1)} %cv_hbm.1, bf16[256,128]{1,0:T(8,128)(2,1)} %cg_hbm.1, s32[1,256]{1,0:T(1,128)} %bitcast.7, bf16[31,128]{1,0:T(8,128)(2,1)} %ck_hbm.1, bf16[1,128]{1,0:T(2,128)(2,1)} %bitcast.8, bf16[256,128]{1,0:T(8,128)(2,1)} %res_hbm.1, s32[2,256]{1,0:T(2,128)} %bitcast.5, ...), custom_call_target="tpu_custom_call" | custom-call | tf_op jit(solution)/shard_map/layer/pallas_call | solution.py:592
  103.3 1.5 %copy.15 = bf16[256,128]{1,0:T(8,128)(2,1)} copy(bf16[256,128]{1,0:T(8,128)(2,1)} %layer.1) | data formatting | bytes 131072

commit v4 on v3

--- a/solution.py
+++ b/solution.py
@@ -29,18 +29,22 @@
 SLOTS = EXPERTS * CAP
 NZ = 16
 G1 = 2
+STEPS1 = (1, -1)
+STEPS2 = (1, -1, 1, -1, 1, -1)
 R1 = ROWS // G1 // 2
-SIZES = (2, 4, 4, 4, 2)
+SIZES = (2, 4, 4, 3, 2, 1)
 G2 = len(SIZES)
 BIG = 2 * max(SIZES) * CAP
-REACH = (0, 1, 15, 2, 12, 5, 11, 6, 10, 7, 9, 8, 14, 3, 13, 4)
+REACH = (15, 2, 14, 3, 12, 5, 11, 6, 10, 7, 9, 8, 13, 4, 0, 1)
+SELF = 2 * REACH.index(0)
 ORDER = (
     0, 1, 10, 11, 100, 101, 20, 21, 110, 111, 200, 201,
     30, 31, 120, 121, 210, 211, 300, 40, 41, 130, 131, 220,
-    221, 310, 140, 141, 230, 231, 400, 401, 320, 240, 241, 410,
-    411, 330, 500, 501, 420, 421, 340, 510, 511, 600, 601, 430,
-    431, 520, 521, 610, 611, 440, 441, 530, 531, 620, 621, 540,
-    541, 630, 631, 640, 641,
+    221, 310, 400, 401, 50, 51, 140, 141, 230, 231, 320, 410,
+    411, 500, 501, 150, 151, 240, 241, 330, 420, 421, 510, 511,
+    600, 601, 250, 251, 340, 430, 431, 520, 521, 610, 611, 350,
+    440, 441, 530, 531, 620, 621, 450, 451, 540, 541, 630, 631,
+    550, 551, 640, 641, 650, 651,
 )
 
 
@@ -303,9 +307,9 @@
         remote(stat.at[me_tp], stat.at[me_tp], stsend.at[k], strecv.at[k], tp_peer(k)).start()
         return carry
 
-    def ring(part, g, rows, first):
+    def ring(part, g, rows, first, steps):
         mm, mj = (x, y) if part == 0 else (y, x)
-        step = 1 - 2 * (g % 2)
+        step = steps[g]
 
         def at(base, by):
             return lax.rem(base + by * step + 2 * RING, RING)
@@ -338,30 +342,30 @@
         d.start()
         flying[key] = d
 
-    def make_gather(buf, rows, first, ssem, rsem):
+    def make_gather(buf, rows, first, steps, ssem, rsem):
         def move(g, part, kind, cols, dev):
             ref = buf.at[pl.ds(first(g, part), rows(g)), cols]
             return remote(ref, ref, ssem.at[part, kind], rsem.at[g, part, kind], dev)
 
         def own(g, part):
-            minor, _, block, _, _, _ = ring(part, g, rows, first)
+            minor, _, block, _, _, _ = ring(part, g, rows, first, steps)
             for kind, by in enumerate((1, -1, 2)):
                 push(ssem, part, kind, move(g, part, kind, block(0), minor(by)))
 
         def sets(g, part):
-            minor, major, block, wide, _, _ = ring(part, g, rows, first)
+            minor, major, block, wide, _, _ = ring(part, g, rows, first, steps)
             for kind, by in enumerate((-1, 1, 2)):
                 move(g, part, kind, block(by), minor(1)).wait_recv()
             push(ssem, part, 3, move(g, part, 3, wide(0), major(1)))
             push(ssem, part, 4, move(g, part, 4, wide(0), major(-1)))
 
         def relay(g, part):
-            _, major, _, wide, _, _ = ring(part, g, rows, first)
+            _, major, _, wide, _, _ = ring(part, g, rows, first, steps)
             move(g, part, 3, wide(-1), major(1)).wait_recv()
             push(ssem, part, 5, move(g, part, 5, wide(-1), major(1)))
 
         def landed(g, part):
-            _, major, _, wide, _, _ = ring(part, g, rows, first)
+            _, major, _, wide, _, _ = ring(part, g, rows, first, steps)
             move(g, part, 4, wide(1), major(1)).wait_recv()
             move(g, part, 5, wide(2), major(1)).wait_recv()
 
@@ -370,7 +374,7 @@
     def first1(g, part):
         return g * 2 * R1 + part * R1
 
-    own1, sets1, relay1, landed1 = make_gather(xg, rows1, first1, ssem1, rsem1)
+    own1, sets1, relay1, landed1 = make_gather(xg, rows1, first1, STEPS1, ssem1, rsem1)
     moves1 = [(g, part) for g in range(G1) for part in range(2)]
     for g, part in moves1:
         own1(g, part)
@@ -386,9 +390,9 @@
         d.wait_recv()
         return carry
 
+    for g, part in moves1:
+        relay1(g, part)
     lax.fori_loop(1, NTP, wait_stat, 0)
-    for g, part in moves1[:2]:
-        relay1(g, part)
 
     means = [stat[j, 0:1, :] for j in range(NTP)]
     mean = sum(means) * (1.0 / NTP)
@@ -422,9 +426,7 @@
 
         lax.fori_loop(0, R1 // 16, some, 0)
 
-    for i, (g, part) in enumerate(moves1):
-        if i + 2 < len(moves1):
-            relay1(*moves1[i + 2])
+    for g, part in moves1:
         normalise(g, part)
     spread_word(4)
 
@@ -449,16 +451,18 @@
         part = PLACE[r][1]
         return x2g.at[pl.ds(r * CAP, CAP), pl.ds(own_pos[part], LANES)]
 
-    for r in range(1, EXPERTS):
+    for r in (*range(SELF), *range(SELF + 1, EXPERTS)):
         dev = along(-REACH[r // 2], lax.rem(c + r, 2))
         remote(dsp.at[dev[0] * 2 + dev[1]], here(r), dsend, drecv.at[PLACE[r][0] * 2 + PLACE[r][1]], dev).start()
-    x2g[:CAP, pl.ds(own_pos[0], LANES)] = dsp[me_sp]
-
-    own2, sets2, relay2, landed2 = make_gather(x2g, rows2, first2, ssem2, rsem2)
+    x2g[SELF * CAP : (SELF + 1) * CAP, pl.ds(own_pos[PLACE[SELF][1]], LANES)] = dsp[me_sp]
+
+    own2, sets2, relay2, landed2 = make_gather(x2g, rows2, first2, STEPS2, ssem2, rsem2)
 
     def arrived(g, part):
-        rows = rows2(g) - CAP if g + part == 0 else rows2(g)
-        ref = x2g.at[pl.ds(first2(g, part), rows), pl.ds(own_pos[part], LANES)]
+        less = CAP if (g, part) == PLACE[SELF] else 0
+        ref = x2g.at[
+            pl.ds(first2(g, part) + less, rows2(g) - less), pl.ds(own_pos[part], LANES)
+        ]
         pltpu.make_async_copy(ref, ref, drecv.at[g * 2 + part]).wait()
         own2(g, part)
 
@@ -506,7 +510,7 @@
                     count:, i * LANES : (i + 1) * LANES
                 ]
         for part in range(2):
-            _, major, _, wide, _, r = ring(part, g, rows2, first2)
+            _, major, _, wide, _, r = ring(part, g, rows2, first2, STEPS2)
             send(g, part, 6, part_sum.at[r, wide(2)], t1.at[r], major(1))
             send(g, part, 7, part_sum.at[r, wide(-1)], v1.at[r], major(-1))
 
@@ -514,13 +518,13 @@
         push(ssem2, part, kind, exchange(g, part, kind, src, dst, dev))
 
     def pass_on(g, part):
-        _, major, _, wide, _, r = ring(part, g, rows2, first2)
+        _, major, _, wide, _, r = ring(part, g, rows2, first2, STEPS2)
         exchange(g, part, 6, t1.at[r], t1.at[r], major(1)).wait_recv()
         s1[r, :] = (t1[r, :].astype(F32) + part_sum[r, wide(1)].astype(F32)).astype(BF16)
         send(g, part, 8, s1.at[r], u1.at[r], major(1))
 
     def ring_sum(g, part):
-        minor, major, _, wide, small, r = ring(part, g, rows2, first2)
+        minor, major, _, wide, small, r = ring(part, g, rows2, first2, STEPS2)
         exchange(g, part, 7, v1.at[r], v1.at[r], major(1)).wait_recv()
         exchange(g, part, 8, u1.at[r], u1.at[r], major(1)).wait_recv()
         q1[r, :] = (
@@ -530,7 +534,7 @@
             send(g, part, kind, q1.at[r, small(by)], dst.at[r], minor(by))
 
     def last_sum(g, part):
-        minor, _, _, _, small, r = ring(part, g, rows2, first2)
+        minor, _, _, _, small, r = ring(part, g, rows2, first2, STEPS2)
         total = q1[r, small(0)].astype(F32)
         for kind, dst in ((9, t2), (10, v2), (11, u2)):
             exchange(g, part, kind, dst.at[r], dst.at[r], minor(1)).wait_recv()
@@ -539,7 +543,7 @@
         ).astype(BF16)
         for i in range(SIZES[g]):
             k = first_chunk(g, part) + i
-            if k > 0:
+            if k != SELF:
                 dev = along(REACH[k // 2], lax.rem(c + k, 2))
                 src = fin.at[pl.ds(k * CAP, CAP), :]
                 remote(src, ret.at[me_sp], rsend, rrecv, dev).start()
@@ -547,7 +551,7 @@
     moves2 = (arrived, sets2, relay2, expert_stage, pass_on, ring_sum, last_sum)
     for code in ORDER:
         moves2[code // 100](code // 10 % 10, code % 10)
-    ret[me_sp] = fin[:CAP, :]
+    ret[me_sp] = fin[SELF * CAP : (SELF + 1) * CAP, :]
 
     for d in flying.values():
         d.wait_send()

time: 105 us -> 103 us (0.981)
    pallas_call x1, Pallas kernels: 103 us -> 102 us  [per_device(): pl.pallas_call(kernel, out_shape=jax.ShapeDtypeStruct((ROWS, LANES), BF16...]
where the time goes in v4:
time: 103 us
  Pallas kernels  102 us (99%)
  local copies, waits for them, and re-layouts  1.47 us (1%)
    pallas_call x1, Pallas kernels, per_device(): pl.pallas_call(kernel, out_shape=jax.ShapeDtypeStruct((ROWS, LANES), BF16...  102 us

profile of v4, /device:TPU:1, one launch (start us, length us, event | category | flops | bytes accessed | tf_op | source)
XLA Modules:
  0.0 103.1 jit_solution(14399021289540591800)
XLA Ops:
  0.0 101.6 %layer.1 = bf16[256,128]{1,0:T(8,128)(2,1)} custom-call(bf16[256,128]{1,0:T(8,128)(2,1)} %cv_hbm.1, bf16[256,128]{1,0:T(8,128)(2,1)} %cg_hbm.1, s32[1,256]{1,0:T(1,128)} %bitcast.7, bf16[31,128]{1,0:T(8,128)(2,1)} %ck_hbm.1, bf16[1,128]{1,0:T(2,128)(2,1)} %bitcast.8, bf16[256,128]{1,0:T(8,128)(2,1)} %res_hbm.1, s32[2,256]{1,0:T(2,128)} %bitcast.5, ...), custom_call_target="tpu_custom_call" | custom-call | tf_op jit(solution)/shard_map/layer/pallas_call | solution.py:596
  101.6 1.5 %copy.15 = bf16[256,128]{1,0:T(8,128)(2,1)} copy(bf16[256,128]{1,0:T(8,128)(2,1)} %layer.1) | data formatting | bytes 131072
